TPU v7x, 128 devices: a whole 4x4x4 slice. The times are simulated.
128 devices in a mesh: fs: 16 (over z, x), tp: 8 (over y, core).
Axes of the slice: x: 4, y: 4, z: 4, core: 2. Of those that a mesh axis runs over, the one named last changes fastest.
Arguments:
- prompts: bfloat16 [8, 1024, 2048], P('tp'), may hold values from -6 to 6
- gain_first: float32 [2048], P('fs'), may hold values from 0.1 to 1.9
- gate_first: float32 [2048, 5632], P('fs', 'tp'), may hold values from -0.125 to 0.125
- up_first: float32 [2048, 5632], P('fs', 'tp'), may hold values from -0.125 to 0.125
- down_first: float32 [5632, 2048], P('fs', 'tp'), may hold values from -0.078125 to 0.078125
- gain_second: float32 [2048], P('fs'), may hold values from 0.1 to 1.9
- gate_second: float32 [2048, 5632], P('fs', 'tp'), may hold values from -0.125 to 0.125
- up_second: float32 [2048, 5632], P('fs', 'tp'), may hold values from -0.125 to 0.125
- down_second: float32 [5632, 2048], P('fs', 'tp'), may hold values from -0.078125 to 0.078125
Outputs:
- served_gate_first: bfloat16 [2048, 5632], P(None, 'fs')
- served_up_first: bfloat16 [2048, 5632], P(None, 'fs')
- served_down_first: bfloat16 [5632, 2048], P('fs')
- served_gate_second: bfloat16 [2048, 5632], P(None, 'fs')
- served_up_second: bfloat16 [2048, 5632], P(None, 'fs')
- served_down_second: bfloat16 [5632, 2048], P('fs')
- prompt_states: bfloat16 [8, 1024, 2048], P('tp', 'fs')
All inputs are finite; a program needn't handle non-finite values.
Results may differ from a plain program's by a relative error of at most 0.012.
Values may be sent and summed in bfloat16 or wider, within the bound.
A program may use at most 128 MiB of HBM per device.

v0:
```python
import jax
import jax.numpy as jnp
from jax import lax
from jax.sharding import Mesh
from jax.sharding import PartitionSpec as P

FS = ("fs_0", "fs_1")


def in_one_piece(arrays, axis, dim, along):
    both = jnp.concatenate(arrays, axis=along)
    out, at, gathered = (lax.all_gather(both, axis, axis=dim, tiled=True), 0, [])
    for a in arrays:
        gathered.append(lax.slice_in_dim(out, at, at + a.shape[along], axis=along))
        at += a.shape[along]
    return tuple(gathered)


def own_rows(terms, axes):
    so_far = terms.astype(jnp.bfloat16)
    for axis in axes:
        so_far = lax.psum_scatter(so_far, axis, scatter_dimension=0, tiled=True)
    return so_far.astype(jnp.float32)


def normalize(row_block):
    widened = row_block.astype(jnp.float32)
    scaled = widened * lax.rsqrt(jnp.mean(widened * widened, axis=-1, keepdims=True) + 1e-06)
    return scaled.astype(jnp.bfloat16)


def activate(normed, gate_cols, up_cols):
    gate_val = jnp.dot(normed, gate_cols, preferred_element_type=jnp.float32)
    up_val = jnp.dot(normed, up_cols, preferred_element_type=jnp.float32)
    return (jax.nn.silu(gate_val) * up_val).astype(jnp.bfloat16)


def per_device(
    prompts,
    gain_first,
    gate_first,
    up_first,
    down_first,
    gain_second,
    gate_second,
    up_second,
    down_second,
):
    fold_gate_a = (gain_first[:, None] * gate_first).astype(jnp.bfloat16)
    fold_up_a = (gain_first[:, None] * up_first).astype(jnp.bfloat16)
    fold_gate_b = (gain_second[:, None] * gate_second).astype(jnp.bfloat16)
    fold_up_b = (gain_second[:, None] * up_second).astype(jnp.bfloat16)
    round_down_a = down_first.astype(jnp.bfloat16)
    round_down_b = down_second.astype(jnp.bfloat16)
    full_rows = (
        *in_one_piece((fold_gate_a, fold_up_a, fold_gate_b, fold_up_b), "tp", 1, 0),
        *in_one_piece((round_down_a, round_down_b), "tp", 1, 0),
    )
    gate_a, up_a, gate_b, up_b = (
        lax.all_to_all(full_rows[0], FS, split_axis=1, concat_axis=0, tiled=True),
        lax.all_to_all(full_rows[1], FS, split_axis=1, concat_axis=0, tiled=True),
        lax.all_to_all(full_rows[2], FS, split_axis=1, concat_axis=0, tiled=True),
        lax.all_to_all(full_rows[3], FS, split_axis=1, concat_axis=0, tiled=True),
    )
    down_a = full_rows[4]
    down_b = full_rows[5]
    tokens_in = prompts.reshape(-1, prompts.shape[-1])
    share = tokens_in.shape[0] // lax.axis_size(FS)
    act_first = activate(normalize(tokens_in), gate_a, up_a)
    selected = act_first
    summed = lax.psum(
        jnp.dot(selected, down_a, preferred_element_type=jnp.float32).astype(jnp.bfloat16), FS
    ).astype(jnp.float32)
    middle_all = (tokens_in.astype(jnp.float32) + 0.5 * summed).astype(jnp.bfloat16)
    act_second = activate(normalize(middle_all), gate_b, up_b)
    middle = lax.dynamic_slice_in_dim(middle_all, lax.axis_index(FS) * share, share, 0)
    selected = act_second
    final_sum = own_rows(jnp.dot(selected, down_b, preferred_element_type=jnp.float32), FS)
    finished = (middle.astype(jnp.float32) + 0.5 * final_sum).astype(jnp.bfloat16)
    return (
        gate_a,
        up_a,
        down_a,
        gate_b,
        up_b,
        down_b,
        finished.reshape(prompts.shape[0], share, prompts.shape[-1]),
    )


def solution(mesh):
    split = Mesh(mesh.devices.reshape(4, 4, mesh.shape["tp"]), ("fs_0", "fs_1", "tp"))
    placed = (
        P("tp", None, None),
        P(FS),
        P(FS, "tp"),
        P(FS, "tp"),
        P(FS, "tp"),
        P(FS),
        P(FS, "tp"),
        P(FS, "tp"),
        P(FS, "tp"),
    )
    return jax.shard_map(
        per_device,
        mesh=split,
        in_specs=placed,
        out_specs=(
            P(None, FS),
            P(None, FS),
            P(FS, None),
            P(None, FS),
            P(None, FS),
            P(FS, None),
            P("tp", FS, None),
        ),
        check_vma=False,
    )
```

profile of v0, /device:TPU:1, one launch (start us, length us, event | category | flops | bytes accessed | tf_op | source)
XLA Modules:
  0.0 340.8 jit_solution(8970967556603132843)
XLA Ops:
  7.2 1.5 multiply_convert_fusion.1
  10.8 41.7 %all-gather.3.cloned.1.call-done = bf16[512,5632]{0,1:T(8,128)(2,1)} async-done(((bf16[512,704]{0,1:T(8,128)(2,1)}), bf16[512,5632]{0,1:T(8,128)(2,1)}) %all-gather.3.cloned.1.call-update) | async-done | bytes 5767184 | tf_op jit(solution)/shard_map/all_gather | solution.py:12
  52.5 5.3 %fusion.38 = (bf16[128,5632]{0,1:T(8,128)(2,1)}, bf16[128,5632]{0,1:T(8,128)(2,1)}, bf16[128,5632]{0,1:T(8,128)(2,1)}, bf16[128,5632]{0,1:T(8,128)(2,1)}) fusion(bf16[512,5632]{0,1:T(8,128)(2,1)} %all-gather.3.cloned.1.call-done), kind=kLoop, calls=%fused_computation.40 | loop fusion | bytes 11534336 | tf_op jit(solution)/shard_map/slice | solution.py:14
  57.9 6.7 %all-to-all-start = ((bf16[128,16,352]{0,2,1:T(8,128)(2,1)}), bf16[128,16,352]{0,2,1:T(8,128)(2,1)S(1)}, u32[]{:S(2)}, u32[]{:S(2)}) async-start(bf16[128,16,352]{0,2,1:T(8,128)(2,1)} %bitcast), calls=%async_computation | async-start | bytes 2883584 | tf_op jit(solution)/shard_map/all_to_all | solution.py:60
  64.5 3.2 fusion.4
  67.8 19.2 %all-to-all-done = bf16[128,16,352]{0,2,1:T(8,128)(2,1)S(1)} async-done(((bf16[128,16,352]{0,2,1:T(8,128)(2,1)}), bf16[128,16,352]{0,2,1:T(8,128)(2,1)S(1)}, u32[]{:S(2)}, u32[]{:S(2)}) %all-to-all-start) | async-done | bytes 1441824 | tf_op jit(solution)/shard_map/all_to_all | solution.py:60
  86.9 4.0 %all-to-all-start.1 = ((bf16[128,16,352]{0,2,1:T(8,128)(2,1)}), bf16[128,16,352]{0,2,1:T(8,128)(2,1)S(1)}, u32[]{:S(2)}, u32[]{:S(2)}) async-start(bf16[128,16,352]{0,2,1:T(8,128)(2,1)} %bitcast.59), calls=%async_computation.1 | async-start | bytes 2883584 | tf_op jit(solution)/shard_map/all_to_all | solution.py:61
  91.0 3.9 %fusion.39 = (bf16[352,2048]{1,0:T(8,128)(2,1)}, bf16[352,2048]{1,0:T(8,128)(2,1)}) fusion(bf16[704,2048]{1,0:T(8,128)(2,1)} %all-gather.5.cloned.1.call-done), kind=kLoop, calls=%fused_computation.41 | loop fusion | bytes 5767168 | tf_op jit(solution)/shard_map/slice | solution.py:14
  95.1 1.1 copy-done.3
  96.2 3.0 fusion.10
  99.2 11.6 %all-to-all-done.1 = bf16[128,16,352]{0,2,1:T(8,128)(2,1)S(1)} async-done(((bf16[128,16,352]{0,2,1:T(8,128)(2,1)}), bf16[128,16,352]{0,2,1:T(8,128)(2,1)S(1)}, u32[]{:S(2)}, u32[]{:S(2)}) %all-to-all-start.1) | async-done | bytes 1441824 | tf_op jit(solution)/shard_map/all_to_all | solution.py:61
  110.9 9.5 %convolution_convert_fusion.1 = bf16[1024,2048]{1,0:T(8,128)(2,1)} fusion(bf16[352,2048]{1,0:T(8,128)(2,1)} %get-tuple-element.14, bf16[2048,352]{0,1:T(8,128)(2,1)S(1)} %copy_bitcast_fusion.2, bf16[1,1024,2048]{2,1,0:T(8,128)(2,1)} %param.9, f32[1024]{0:T(1024)S(1)} %add_rsqrt_fusion.1, f32[1024,352]{0,1:T(8,128)} %fusion.10), kind=kOutput, calls=%fused_computation.13 | convolution fusion | flops 2963341312 | bytes 12718080 | tf_op jit(solution)/shard_map/dot_general | solution.py:72
  120.5 1.3 copy-done.1
  121.8 41.3 %all_to_all.76 = bf16[128,16,352]{0,2,1:T(8,128)(2,1)S(1)} all-to-all(bf16[128,16,352]{0,2,1:T(8,128)(2,1)S(1)} %bitcast.58), channel_id=1, replica_groups=mesh['fs_0'=4,'fs_1'=4,'tp'=8] {'fs_0','fs_1'}, dimensions={1} | all-to-all | bytes 2883584 | tf_op jit(solution)/shard_map/all_to_all | solution.py:62
  163.1 3.7 %all-to-all-start.3 = ((bf16[128,16,352]{0,2,1:T(8,128)(2,1)}), bf16[128,16,352]{0,2,1:T(8,128)(2,1)S(1)}, u32[]{:S(2)}, u32[]{:S(2)}) async-start(bf16[128,16,352]{0,2,1:T(8,128)(2,1)} %bitcast.57), calls=%async_computation.3 | async-start | bytes 2883584 | tf_op jit(solution)/shard_map/all_to_all | solution.py:63
  167.1 1.3 copy_bitcast_fusion.1
  168.4 20.0 %all-to-all-done.3 = bf16[128,16,352]{0,2,1:T(8,128)(2,1)S(1)} async-done(((bf16[128,16,352]{0,2,1:T(8,128)(2,1)}), bf16[128,16,352]{0,2,1:T(8,128)(2,1)S(1)}, u32[]{:S(2)}, u32[]{:S(2)}) %all-to-all-start.3) | async-done | bytes 1441824 | tf_op jit(solution)/shard_map/all_to_all | solution.py:63
  188.6 55.8 %all-reduce.2.cloned.1.call-done = bf16[1024,2048]{1,0:T(8,128)(2,1)} async-done(((bf16[1024,2048]{1,0:T(8,128)(2,1)}), bf16[1024,2048]{1,0:T(8,128)(2,1)}) %all-reduce.2.cloned.1.call-update) | async-done | bytes 4194320 | tf_op jit(solution)/shard_map/psum | solution.py:71
  244.4 4.6 %fusion.2 = (f32[1024]{0:T(1024)S(1)}, bf16[1024,2048]{1,0:T(8,128)(2,1)S(1)}) fusion(bf16[1024,2048]{1,0:T(8,128)(2,1)} %all-reduce.2.cloned.1.call-done, bf16[1,1024,2048]{2,1,0:T(8,128)(2,1)} %param.9), kind=kLoop, calls=%fused_computation.6 | loop fusion | flops 16776192 | bytes 12587008 | tf_op jit(solution)/shard_map/reduce_sum | solution.py:28
  249.1 2.9 fusion.14
  252.0 9.0 %convolution_convert_fusion = bf16[1024,2048]{1,0:T(8,128)(2,1)} fusion(bf16[352,2048]{1,0:T(8,128)(2,1)} %get-tuple-element.13, bf16[2048,352]{0,1:T(8,128)(2,1)S(1)} %copy_bitcast_fusion, bf16[1024,2048]{1,0:T(8,128)(2,1)} %copy-done.2, f32[1024]{0:T(1024)S(1)} %add_rsqrt_fusion, f32[1024,352]{0,1:T(8,128)} %fusion.14), kind=kOutput, calls=%fused_computation.12 | convolution fusion | flops 2963341312 | bytes 12718080 | tf_op jit(solution)/shard_map/dot_general | solution.py:78
  261.1 47.2 %reduce-scatter.3.cloned.1.call-done = bf16[256,2048]{1,0:T(8,128)(2,1)} async-done(((bf16[1024,2048]{1,0:T(8,128)(2,1)}), bf16[256,2048]{1,0:T(8,128)(2,1)}) %reduce-scatter.3.cloned.1.call-update) | async-done | bytes 1048592 | tf_op jit(solution)/shard_map/reduce_scatter | solution.py:22
  308.3 24.1 %reduce-scatter.5.cloned.1.call-done = bf16[64,2048]{1,0:T(8,128)(2,1)} async-done(((bf16[256,2048]{1,0:T(8,128)(2,1)}), bf16[64,2048]{1,0:T(8,128)(2,1)}) %reduce-scatter.5.cloned.1.call-update) | async-done | bytes 262160 | tf_op jit(solution)/shard_map/reduce_scatter | solution.py:22
  332.4 1.8 fusion.34
  (36 shorter events, 3.1 us)
Async XLA Ops:
  7.2 45.4 %all-gather.3.cloned.1.call-start = ((), (), s32[]{:S(2)}) async-start(), calls=%async_computation.6 | async-start | bytes 6488064 | tf_op jit(solution)/shard_map/all_gather | solution.py:12
  8.7 1.0 copy-start.7
  8.7 1.3 copy-start.8
  9.7 81.3 %all-gather.5.cloned.1.call-start = ((), (), s32[]{:S(2)}) async-start(), calls=%async_computation.7 | async-start | bytes 3244032 | tf_op jit(solution)/shard_map/all_gather | solution.py:12
  57.9 29.1 %all-to-all-start = ((bf16[128,16,352]{0,2,1:T(8,128)(2,1)}), bf16[128,16,352]{0,2,1:T(8,128)(2,1)S(1)}, u32[]{:S(2)}, u32[]{:S(2)}) async-start(bf16[128,16,352]{0,2,1:T(8,128)(2,1)} %bitcast), calls=%async_computation | async-start | bytes 2883584 | tf_op jit(solution)/shard_map/all_to_all | solution.py:60
  86.9 23.8 %all-to-all-start.1 = ((bf16[128,16,352]{0,2,1:T(8,128)(2,1)}), bf16[128,16,352]{0,2,1:T(8,128)(2,1)S(1)}, u32[]{:S(2)}, u32[]{:S(2)}) async-start(bf16[128,16,352]{0,2,1:T(8,128)(2,1)} %bitcast.59), calls=%async_computation.1 | async-start | bytes 2883584 | tf_op jit(solution)/shard_map/all_to_all | solution.py:61
  90.9 153.5 %all-reduce.2.cloned.1.call-start = ((), (), s32[]{:S(2)}) async-start(), calls=%async_computation.8 | async-start | bytes 8388608 | tf_op jit(solution)/shard_map/psum | solution.py:71
  91.0 5.2 %copy-start = (bf16[1,1024,2048]{2,1,0:T(8,128)(2,1)S(1)}, bf16[1,1024,2048]{2,1,0:T(8,128)(2,1)}, u32[]{:S(2)}) copy-start(bf16[1,1024,2048]{2,1,0:T(8,128)(2,1)} %param.9) | copy-start | bytes 12582916
  95.1 1.1 copy-start.3
  110.9 9.5 %copy-start.4 = (bf16[2048,352]{0,1:T(8,128)(2,1)}, bf16[2048,352]{0,1:T(8,128)(2,1)S(1)}, u32[]{:S(2)}) copy-start(bf16[2048,352]{0,1:T(8,128)(2,1)S(1)} %copy_bitcast_fusion.2) | copy-start | bytes 4325380
  120.5 1.4 copy-start.1
  163.1 25.3 %all-to-all-start.3 = ((bf16[128,16,352]{0,2,1:T(8,128)(2,1)}), bf16[128,16,352]{0,2,1:T(8,128)(2,1)S(1)}, u32[]{:S(2)}, u32[]{:S(2)}) async-start(bf16[128,16,352]{0,2,1:T(8,128)(2,1)} %bitcast.57), calls=%async_computation.3 | async-start | bytes 2883584 | tf_op jit(solution)/shard_map/all_to_all | solution.py:63
  166.8 141.4 %reduce-scatter.3.cloned.1.call-start = ((), (), s32[]{:S(2)}) async-start(), calls=%async_computation.9 | async-start | bytes 5242880 | tf_op jit(solution)/shard_map/reduce_scatter | solution.py:22
  188.6 63.4 %copy-start.6 = (bf16[2048,352]{0,1:T(8,128)(2,1)}, bf16[2048,352]{0,1:T(8,128)(2,1)S(1)}, u32[]{:S(2)}) copy-start(bf16[2048,352]{0,1:T(8,128)(2,1)S(1)} %copy_bitcast_fusion) | copy-start | bytes 4325380
  188.6 60.5 %copy-start.5 = (bf16[2048,352]{0,1:T(8,128)(2,1)S(1)}, bf16[2048,352]{0,1:T(8,128)(2,1)}, u32[]{:S(2)}) copy-start(bf16[2048,352]{0,1:T(8,128)(2,1)} %copy_bitcast_fusion.1) | copy-start | bytes 4325380
  249.1 3.0 copy-start.2
  261.0 71.4 %reduce-scatter.5.cloned.1.call-start = ((), (), s32[]{:S(2)}) async-start(), calls=%async_computation.10 | async-start | bytes 1310720 | tf_op jit(solution)/shard_map/reduce_scatter | solution.py:22
Sparse Core Ops, SparseCore 0:
  10.2 42.2 all-gather.2
  54.8 30.0 all-gather.4
  120.6 123.7 all-reduce.1
  261.2 47.0 reduce-scatter.2
  310.5 21.8 reduce-scatter.4
where the time goes:
time: 342 us; the launch traced here: 341 us
  waiting for transfers between devices  220 us (64%)
  blocking collectives  41.3 us (12%)
  matrix products  24.5 us (7%)
  starting transfers between devices  14.7 us (4%)
  between operations  14 us (4%)
  local copies, waits for them, and re-layouts  13.8 us (4%)
  other arithmetic  12.8 us (4%)
    reduce_scatter x2, waiting for transfers between devices, own_rows(): so_far = lax.psum_scatter(so_far, axis, scatter_dimension=0, tiled=True)  71.3 us
    psum x1, waiting for transfers between devices, per_device(): lax.psum(jnp.dot(selected, down_a, preferred_element_type=jnp.float32).as...  55.8 us
    all_gather x2, waiting for transfers between devices, in_one_piece(): lax.all_gather(both, axis, axis=dim, tiled=True)  41.7 us
    all_to_all x1, blocking collectives, per_device(): lax.all_to_all(full_rows[2], FS, split_axis=1, concat_axis=0, tiled=True)  41.3 us
    all_to_all x1, waiting for transfers between devices, per_device(): lax.all_to_all(full_rows[3], FS, split_axis=1, concat_axis=0, tiled=True)  20 us
    all_to_all x1, waiting for transfers between devices, per_device(): lax.all_to_all(full_rows[0], FS, split_axis=1, concat_axis=0, tiled=True)  19.2 us
    all_to_all x1, waiting for transfers between devices, per_device(): lax.all_to_all(full_rows[1], FS, split_axis=1, concat_axis=0, tiled=True)  11.6 us
    dot_general x1, matrix products, per_device(): jnp.dot(selected, down_a, preferred_element_type=jnp.float32)  9.5 us
  transfers between devices with their start and end apart: 8, of which 7 were waited for; matrix products, arithmetic and copies ran while one was open for 5% of the time, Pallas kernels for 0%

commit v1 on v0

v1 whole, which is shorter than its diff:
```python
import functools

import jax
import jax.numpy as jnp
from jax import lax
from jax.experimental import pallas as pl
from jax.experimental.pallas import tpu as pltpu
from jax.sharding import PartitionSpec as P

D = 2048
FF = 5632
HB = 352
HP = 384
TOK = 1024
MESH = pl.DeviceIdType.MESH
BF = jnp.bfloat16
F32 = jnp.float32


def rem4(v):
    return lax.rem(v, 4)


def kernel(
    x_hbm, wt, dn,
    gu1_o, gu2_o, d1_o, d2_o, ps_o,
    nx, ng, xown, mid, gu, dd, act, part,
    r2, ra, rb, tt, acc, sb, q2, qa, qb, qt, ost,
    w_recv, w_a, w_f, w_s, d_recv, d_send, d_loc, rs_send, rs_recv, ag_send, ag_recv, x_sem, o_sem,
):
    f = lax.axis_index("fs")
    t = lax.axis_index("tp")
    z = lax.div(f, 4)
    x = lax.rem(f, 4)
    y = lax.div(t, 2)
    core = lax.rem(t, 2)
    sib = (f, 2 * y + 1 - core)
    pending = []

    def send(src, dst, ssem, rsem, dev, cond=None):
        cp = pltpu.make_async_remote_copy(
            src_ref=src, dst_ref=dst, send_sem=ssem, recv_sem=rsem, device_id=dev, device_id_type=MESH
        )
        if cond is None:
            cp.start()
        else:
            pl.when(cond)(cp.start)
        pending.append((cp, cond))

    def drain():
        for cp, cond in pending:
            if cond is None:
                cp.wait_send()
            else:
                pl.when(cond)(cp.wait_send)
        pending.clear()

    def arrived(dst, sem):
        pltpu.make_async_copy(dst, dst, sem).wait()

    xcp = []
    for r in range(4):
        cp = pltpu.make_async_copy(x_hbm.at[r], nx.at[r], x_sem.at[r])
        cp.start()
        xcp.append(cp)
    own_in = pltpu.make_async_copy(x_hbm.at[z, x], xown, x_sem.at[4])
    own_in.start()

    def wrows(h, ft):
        return gu.at[h, pl.ds(pl.multiple_of(ft * 128, 128), 128), :]

    def stage_a(h):
        for g in range(2):
            df = 2 * t + g
            dt = 2 * y + lax.rem(f, 2)
            same = jnp.logical_and(df == f, dt == t)
            other = jnp.logical_not(same)
            send(wt.at[h, g], wrows(h, f), w_a.at[h, g], w_recv.at[h, f], (df, dt), other)

            @pl.when(same)
            def _():
                pltpu.make_async_copy(wt.at[h, g], wrows(h, f), w_recv.at[h, f]).start()

    ny = rem4(y + 1 + 2 * core)
    dist = rem4(jnp.where(core == 0, y - z, z - y) + 4)
    ORDER = [(0, 0), (0, 1), (1, 0), (1, 1), (3, 0), (3, 1), (2, 0), (2, 1)]

    def chain(h, i):
        dz, k = ORDER[i]
        ft = 4 * rem4(z + dz) + 2 * k + core
        tile = wrows(h, ft)
        arrived(tile, w_recv.at[h, ft])
        send(tile, tile, w_f.at[h, i], w_recv.at[h, ft], (f, 2 * ny + core), dist < 3)
        send(tile, tile, w_s.at[h, i], w_recv.at[h, ft], sib)

    def chain_other(h):
        for i in range(8):
            ft = 2 * i + 1 - core
            arrived(wrows(h, ft), w_recv.at[h, ft])

    yp, ym, y2 = rem4(y + 1), rem4(y + 3), rem4(y + 2)

    def dblk(h, tb, q):
        return dd.at[h, pl.ds(176 * q, 176), pl.ds(pl.multiple_of(tb * 256, 256), 256)]

    def down_start(h):
        pltpu.make_async_copy(
            dn.at[h], dd.at[h, pl.ds(0, HB), pl.ds(pl.multiple_of(t * 256, 256), 256)], d_loc.at[h]
        ).start()
        k = 0
        for q in range(2):
            src = dn.at[h, pl.ds(176 * q, 176), :]
            for dev in ((f, 2 * yp + core), (f, 2 * ym + core), sib):
                send(src, dblk(h, t, q), d_send.at[h, k], d_recv.at[h, t, q], dev)
                k += 1

    def down_mid(h):
        tm, tp = 2 * ym + core, 2 * yp + core
        arrived(dblk(h, tm, 0), d_recv.at[h, tm, 0])
        send(dblk(h, tm, 0), dblk(h, tm, 0), d_send.at[h, 6], d_recv.at[h, tm, 0], (f, 2 * yp + core))
        arrived(dblk(h, tp, 1), d_recv.at[h, tp, 1])
        send(dblk(h, tp, 1), dblk(h, tp, 1), d_send.at[h, 7], d_recv.at[h, tp, 1], (f, 2 * ym + core))
        send(dblk(h, tm, 0), dblk(h, tm, 0), d_send.at[h, 8], d_recv.at[h, tm, 0], sib)
        send(dblk(h, tp, 1), dblk(h, tp, 1), d_send.at[h, 9], d_recv.at[h, tp, 1], sib)
        k = 10
        for tb, q in ((tm, 1), (tp, 0)):
            arrived(dblk(h, tb, q), d_recv.at[h, tb, q])
            send(dblk(h, tb, q), dblk(h, tb, q), d_send.at[h, k], d_recv.at[h, tb, q], sib)
            k += 1

    def down_end(h):
        t2 = 2 * y2 + core
        for q in range(2):
            arrived(dblk(h, t2, q), d_recv.at[h, t2, q])
            send(dblk(h, t2, q), dblk(h, t2, q), d_send.at[h, 12 + q], d_recv.at[h, t2, q], sib)
        for yy in range(4):
            for q in range(2):
                tb = 2 * yy + 1 - core
                arrived(dblk(h, tb, q), d_recv.at[h, tb, q])
        pltpu.make_async_copy(
            dn.at[h], dd.at[h, pl.ds(0, HB), pl.ds(pl.multiple_of(t * 256, 256), 256)], d_loc.at[h]
        ).wait()

    def norm_rows(v):
        w = v.astype(F32)
        return (w * lax.rsqrt(jnp.mean(w * w, axis=-1, keepdims=True) + 1e-06)).astype(BF)

    def gate_up(src, h):
        @pl.loop(0, 4)
        def _(r):
            a = src[r].reshape(256, D)
            v = jnp.dot(a, gu[h], preferred_element_type=F32)
            gt = v[:, :HP]
            up = v[:, HP:]
            act[r] = (gt * jax.nn.sigmoid(gt) * up).astype(BF).reshape(4, 64, HP)

    def colsl(ab):
        return pl.ds(1024 * ab, 1024)

    def pv(h, ab, idx, q):
        if ab == 0:
            return part.at[h, pl.ds(2 * q, 2), idx, :, colsl(0)]
        return part.at[h, idx, pl.ds(2 * q, 2), :, colsl(1)]

    def dev1(ab, step):
        if ab == 0:
            return (4 * z + rem4(x + step + 4), t)
        return (4 * rem4(z + step + 4) + x, t)

    def me1(ab, step):
        return rem4((x if ab == 0 else z) + step + 4)

    def down_chunk(h, ab, idx):
        w = dd[h, :, 1024 * ab:1024 * ab + 1024]
        if ab == 0:
            a = act[:, pl.ds(idx, 1)].reshape(256, HP)
        else:
            a = act[idx].reshape(256, HP)
        v = jnp.dot(a, w, preferred_element_type=F32).astype(BF)
        if ab == 0:
            part[h, :, pl.ds(idx, 1), :, 0:1024] = v.reshape(4, 1, 64, 1024)
        else:
            part[h, idx, :, :, 1024:2048] = v.reshape(4, 64, 1024)

    def s1(h, ab, k, src, dst, step):
        send(src, dst, rs_send.at[h, 0, ab, k], rs_recv.at[h, 0, ab, k], dev1(ab, step))

    def s2(h, ab, k, src, dst, step):
        send(src, dst, rs_send.at[h, 1, ab, k], rs_recv.at[h, 1, ab, k], dev1(1 - ab, step))

    def rs_first(h, between=None):
        for ab in range(2):
            i2 = me1(ab, 2)
            down_chunk(h, ab, i2)
            s1(h, ab, 0, pv(h, ab, i2, 0), r2.at[h, ab, 0], 1)
            s1(h, ab, 1, pv(h, ab, i2, 1), r2.at[h, ab, 1], -1)
        for ab in range(2):
            ip = me1(ab, 1)
            down_chunk(h, ab, ip)
            s1(h, ab, 3, pv(h, ab, ip, 1), ra.at[h, ab, pl.ds(2, 2)], 1)
        for ab in range(2):
            im = me1(ab, -1)
            down_chunk(h, ab, im)
            s1(h, ab, 4, pv(h, ab, im, 0), rb.at[h, ab, pl.ds(0, 2)], -1)
        for ab in range(2):
            down_chunk(h, ab, me1(ab, 0))

    def rs_second(h):
        for ab in range(2):
            arrived(r2.at[h, ab, 0], rs_recv.at[h, 0, ab, 0])
            tt[h, ab, 0] = (r2[h, ab, 0].astype(F32) + pv(h, ab, me1(ab, 1), 0)[...].astype(F32)).astype(BF)
            s1(h, ab, 2, tt.at[h, ab, 0], ra.at[h, ab, pl.ds(0, 2)], 1)
            arrived(r2.at[h, ab, 1], rs_recv.at[h, 0, ab, 1])
            tt[h, ab, 1] = (r2[h, ab, 1].astype(F32) + pv(h, ab, me1(ab, -1), 1)[...].astype(F32)).astype(BF)
            s1(h, ab, 5, tt.at[h, ab, 1], rb.at[h, ab, pl.ds(2, 2)], -1)

    def rs_third(h):
        for ab in range(2):
            for q in range(2):
                sl = pl.ds(2 * q, 2)
                arrived(ra.at[h, ab, sl], rs_recv.at[h, 0, ab, 2 + q])
                arrived(rb.at[h, ab, sl], rs_recv.at[h, 0, ab, 4 + q])
                s = (
                    pv(h, ab, me1(ab, 0), q)[...].astype(F32)
                    + ra[h, ab, 2 * q:2 * q + 2].astype(F32)
                    + rb[h, ab, 2 * q:2 * q + 2].astype(F32)
                )
                acc[ab, 2 * q:2 * q + 2] = s
                sb[h, ab, 2 * q:2 * q + 2] = s.astype(BF)
            i2, ip, im = me1(1 - ab, 2), me1(1 - ab, 1), me1(1 - ab, -1)
            s2(h, ab, 0, sb.at[h, ab, i2, pl.ds(0, 32)], q2.at[h, ab, 0], 1)
            s2(h, ab, 1, sb.at[h, ab, i2, pl.ds(32, 32)], q2.at[h, ab, 1], -1)
            s2(h, ab, 3, sb.at[h, ab, ip, pl.ds(32, 32)], qa.at[h, ab, pl.ds(32, 32)], 1)
            s2(h, ab, 4, sb.at[h, ab, im, pl.ds(0, 32)], qb.at[h, ab, pl.ds(0, 32)], -1)

    def rs_fourth(h):
        for ab in range(2):
            ip, im = me1(1 - ab, 1), me1(1 - ab, -1)
            arrived(q2.at[h, ab, 0], rs_recv.at[h, 1, ab, 0])
            qt[h, ab, 0] = (q2[h, ab, 0].astype(F32) + acc[ab, ip, 0:32]).astype(BF)
            s2(h, ab, 2, qt.at[h, ab, 0], qa.at[h, ab, pl.ds(0, 32)], 1)
            arrived(q2.at[h, ab, 1], rs_recv.at[h, 1, ab, 1])
            qt[h, ab, 1] = (q2[h, ab, 1].astype(F32) + acc[ab, im, 32:64]).astype(BF)
            s2(h, ab, 5, qt.at[h, ab, 1], qb.at[h, ab, pl.ds(32, 32)], -1)
        out = []
        for ab in range(2):
            for q in range(2):
                arrived(qa.at[h, ab, pl.ds(32 * q, 32)], rs_recv.at[h, 1, ab, 2 + q])
                arrived(qb.at[h, ab, pl.ds(32 * q, 32)], rs_recv.at[h, 1, ab, 4 + q])
            out.append(acc[ab, me1(1 - ab, 0)] + qa[h, ab].astype(F32) + qb[h, ab].astype(F32))
        return jnp.concatenate(out, axis=-1)

    def gv(ab, i, j, rows=None):
        rows = slice(None) if rows is None else rows
        if ab == 0:
            return ng.at[i, j, rows, colsl(0)]
        return ng.at[j, i, rows, colsl(1)]

    def ag(h=0):
        def snd(ab, k, ref, second, step):
            send(ref, ref, ag_send.at[ab, k], ag_recv.at[ab, k], dev1(ab if second else 1 - ab, step))

        idx = []
        for ab in range(2):
            i0 = me1(1 - ab, 0)
            j0 = me1(ab, 0)
            idx.append((i0, j0, rem4(i0 + 1), rem4(i0 + 3), rem4(i0 + 2), rem4(j0 + 1), rem4(j0 + 3), rem4(j0 + 2)))
        lo, hi = pl.ds(0, 32), pl.ds(32, 32)
        for ab in range(2):
            i0, j0 = idx[ab][:2]
            snd(ab, 0, gv(ab, i0, j0), False, 1)
            snd(ab, 1, gv(ab, i0, j0), False, -1)
            snd(ab, 4, gv(ab, i0, j0), True, 1)
            snd(ab, 8, gv(ab, i0, j0), True, -1)
        for ab in range(2):
            i0, j0, ip, im, i2, jp, jm, j2 = idx[ab]
            arrived(gv(ab, im, j0), ag_recv.at[ab, 0])
            snd(ab, 2, gv(ab, im, j0, lo), False, 1)
            snd(ab, 7, gv(ab, im, j0), True, 1)
            snd(ab, 11, gv(ab, im, j0), True, -1)
            arrived(gv(ab, ip, j0), ag_recv.at[ab, 1])
            snd(ab, 3, gv(ab, ip, j0, hi), False, -1)
            snd(ab, 5, gv(ab, ip, j0), True, 1)
            snd(ab, 9, gv(ab, ip, j0), True, -1)
        for ab in range(2):
            i0, j0, ip, im, i2, jp, jm, j2 = idx[ab]
            arrived(gv(ab, i0, jm), ag_recv.at[ab, 4])
            snd(ab, 12, gv(ab, i0, jm), True, 1)
            arrived(gv(ab, i0, jp), ag_recv.at[ab, 8])
        for ab in range(2):
            i0, j0, ip, im, i2, jp, jm, j2 = idx[ab]
            arrived(gv(ab, i2, j0, lo), ag_recv.at[ab, 2])
            arrived(gv(ab, i2, j0, hi), ag_recv.at[ab, 3])
            snd(ab, 6, gv(ab, i2, j0), True, 1)
            snd(ab, 10, gv(ab, i2, j0), True, -1)
        for ab in range(2):
            i0, j0, ip, im, i2, jp, jm, j2 = idx[ab]
            arrived(gv(ab, ip, jm), ag_recv.at[ab, 5])
            snd(ab, 13, gv(ab, ip, jm), True, 1)
            arrived(gv(ab, im, jp), ag_recv.at[ab, 11])
            snd(ab, 14, gv(ab, im, jp), True, -1)
        for ab in range(2):
            i0, j0, ip, im, i2, jp, jm, j2 = idx[ab]
            arrived(gv(ab, im, jm), ag_recv.at[ab, 7])
            arrived(gv(ab, ip, jp), ag_recv.at[ab, 9])
            arrived(gv(ab, i2, jm), ag_recv.at[ab, 6])
            arrived(gv(ab, i2, jp), ag_recv.at[ab, 10])
            snd(ab, 15, gv(ab, i2, jp), True, -1)
        for ab in range(2):
            i0, j0, ip, im, i2, jp, jm, j2 = idx[ab]
            arrived(gv(ab, i0, j2), ag_recv.at[ab, 12])
            arrived(gv(ab, ip, j2), ag_recv.at[ab, 13])
            arrived(gv(ab, im, j2), ag_recv.at[ab, 14])
            arrived(gv(ab, i2, j2), ag_recv.at[ab, 15])

    def put(src, dst, k):
        pltpu.make_async_copy(src, dst, o_sem.at[k]).start()

    def put_wait(src, dst, k):
        pltpu.make_async_copy(src, dst, o_sem.at[k]).wait()

    stage_a(0)
    down_start(0)
    for h in range(2):
        dd[h, HB:HP, :] = jnp.zeros((HP - HB, D), BF)
    for r in range(4):
        xcp[r].wait()
        for k in range(4):
            nx[r, k] = norm_rows(nx[r, k])
    for i in range(4):
        chain(0, i)
    down_mid(0)
    stage_a(1)
    for i in range(4, 8):
        chain(0, i)
    down_end(0)
    chain_other(0)
    put(gu.at[0], gu1_o, 0)
    put(dd.at[0, pl.ds(0, HB)], d1_o, 1)

    gate_up(nx, 0)
    rs_first(0)
    for i in range(2):
        chain(1, i)
    rs_second(0)
    for i in range(2, 8):
        chain(1, i)
    down_start(1)
    rs_third(0)
    chain_other(1)
    down_mid(1)
    branch = rs_fourth(0)
    own_in.wait()
    m = (xown[...].astype(F32) + 0.5 * branch).astype(BF)
    mid[...] = m
    ng[z, x] = norm_rows(m)
    ag()
    down_end(1)
    put(gu.at[1], gu2_o, 2)
    put(dd.at[1, pl.ds(0, HB)], d2_o, 3)

    gate_up(ng, 1)
    rs_first(1)
    rs_second(1)
    rs_third(1)
    branch = rs_fourth(1)
    ost[...] = (mid[...].astype(F32) + 0.5 * branch).astype(BF)
    put(ost, ps_o, 4)

    drain()
    put_wait(gu.at[0], gu1_o, 0)
    put_wait(dd.at[0, pl.ds(0, HB)], d1_o, 1)
    put_wait(gu.at[1], gu2_o, 2)
    put_wait(dd.at[1, pl.ds(0, HB)], d2_o, 3)
    put_wait(ost, ps_o, 4)


def run(xin, wt, dn):
    vm = pltpu.VMEM
    dma = pltpu.SemaphoreType.DMA
    out_shape = (
        jax.ShapeDtypeStruct((D, 2 * HP), BF),
        jax.ShapeDtypeStruct((D, 2 * HP), BF),
        jax.ShapeDtypeStruct((HB, D), BF),
        jax.ShapeDtypeStruct((HB, D), BF),
        jax.ShapeDtypeStruct((64, D), BF),
    )
    scratch = [
        vm((4, 4, 64, D), BF), vm((4, 4, 64, D), BF), vm((64, D), BF), vm((64, D), BF),
        vm((2, D, 2 * HP), BF), vm((2, HP, D), BF), vm((4, 4, 64, HP), BF), vm((2, 4, 4, 64, D), BF),
        vm((2, 2, 2, 2, 64, 1024), BF), vm((2, 2, 4, 64, 1024), BF), vm((2, 2, 4, 64, 1024), BF),
        vm((2, 2, 2, 2, 64, 1024), BF), vm((2, 4, 64, 1024), F32), vm((2, 2, 4, 64, 1024), BF),
        vm((2, 2, 2, 32, 1024), BF), vm((2, 2, 64, 1024), BF), vm((2, 2, 64, 1024), BF),
        vm((2, 2, 2, 32, 1024), BF), vm((64, D), BF),
        dma((2, 16)), dma((2, 2)), dma((2, 8)), dma((2, 8)), dma((2, 8, 2)), dma((2, 14)), dma((2,)),
        dma((2, 2, 2, 6)), dma((2, 2, 2, 6)), dma((2, 16)), dma((2, 16)), dma((5,)), dma((5,)),
    ]
    return pl.pallas_call(
        kernel,
        out_shape=out_shape,
        in_specs=[
            pl.BlockSpec(memory_space=pl.ANY),
            pl.BlockSpec(memory_space=pltpu.VMEM),
            pl.BlockSpec(memory_space=pltpu.VMEM),
        ],
        out_specs=tuple(pl.BlockSpec(memory_space=pl.ANY) for _ in range(5)),
        scratch_shapes=scratch,
        compiler_params=pltpu.CompilerParams(has_side_effects=True, vmem_limit_bytes=62 * 1024 * 1024),
    )(xin, wt, dn)


def tiles(gain, gate, up):
    def one(w):
        v = (gain[:, None] * w).astype(BF).reshape(128, 2, HB).transpose(1, 0, 2)
        return jnp.pad(v, ((0, 0), (0, 0), (0, HP - HB)))

    return jnp.concatenate([one(gate), one(up)], axis=-1)


def per_device(
    prompts, gain_first, gate_first, up_first, down_first, gain_second, gate_second, up_second, down_second
):
    wt = jnp.stack([tiles(gain_first, gate_first, up_first), tiles(gain_second, gate_second, up_second)])
    dn = jnp.stack([down_first.astype(BF), down_second.astype(BF)])
    xin = prompts.reshape(4, 4, 64, D)
    gu1, gu2, d1, d2, ps = run(xin, wt, dn)
    return (
        gu1[:, :HB], gu1[:, HP:HP + HB], d1,
        gu2[:, :HB], gu2[:, HP:HP + HB], d2,
        ps.reshape(1, 64, D),
    )


def solution(mesh):
    w = P("fs", "tp")
    return jax.shard_map(
        per_device,
        mesh=mesh,
        in_specs=(P("tp", None, None), P("fs"), w, w, w, P("fs"), w, w, w),
        out_specs=(
            P(None, "fs"), P(None, "fs"), P("fs", None),
            P(None, "fs"), P(None, "fs"), P("fs", None),
            P("tp", "fs", None),
        ),
        check_vma=False,
    )
```

time: 342 us -> 191 us (0.56)
  waiting for transfers between devices: 220 us -> 0 us
  Pallas kernels: 0 us -> 171 us
  blocking collectives: 41.3 us -> 0 us
  matrix products: 24.5 us -> 0 us
  starting transfers between devices: 14.7 us -> 0 us
  between operations: 14 us -> 0.75 us
  other arithmetic: 12.8 us -> 3.18 us
    pallas_call x0 -> x1, Pallas kernels: none -> 171 us  [run(): pl.pallas_call(kernel, out_shape=out_shape, in_specs=[pl.BlockSpec(memory...]
    reduce_scatter x2 -> x0, waiting for transfers between devices: 71.3 us -> none  [own_rows(): so_far = lax.psum_scatter(so_far, axis, scatter_dimension=0, tiled=True)]
    psum x1 -> x0, waiting for transfers between devices: 55.8 us -> none  [per_device(): lax.psum(jnp.dot(selected, down_a, preferred_element_type=jnp.float32).as...]
    all_to_all x3 -> x0, waiting for transfers between devices: 50.8 us -> none  [the longest x1 20 us: per_device(): lax.all_to_all(full_rows[3], FS, split_axis=1, concat_axis=0, tiled=True)]
    all_gather x2 -> x0, waiting for transfers between devices: 41.7 us -> none  [in_one_piece(): lax.all_gather(both, axis, axis=dim, tiled=True)]
    all_to_all x1 -> x0, blocking collectives: 41.3 us -> none  [per_device(): lax.all_to_all(full_rows[2], FS, split_axis=1, concat_axis=0, tiled=True)]
    dot_general x4 -> x0, matrix products: 24.5 us -> none  [the longest x1 9.5 us: per_device(): jnp.dot(selected, down_a, preferred_element_type=jnp.float32)]
    all_to_all x3 -> x0, starting transfers between devices: 14.3 us -> none  [the longest x1 6.66 us: per_device(): lax.all_to_all(full_rows[0], FS, split_axis=1, concat_axis=0, tiled=True)]
  transfers between devices with their start and end apart: 8 -> 0, of which waited for: 7 -> 0; matrix products, arithmetic and copies ran while one was open for 5% -> 0% of each run, Pallas kernels for 0% -> 0%
where the time goes in v1:
time: 191 us; the launch traced here: 190 us
  Pallas kernels  171 us (90%)
  local copies, waits for them, and re-layouts  15.1 us (8%)
  other arithmetic  3.18 us (2%)
    pallas_call x1, Pallas kernels, run(): pl.pallas_call(kernel, out_shape=out_shape, in_specs=[pl.BlockSpec(memory...  171 us
    unnamed x23, local copies, waits for them, and re-layouts  10 us

profile of v1, /device:TPU:1, one launch (start us, length us, event | category | flops | bytes accessed | tf_op | source)
XLA Modules:
  0.0 190.5 jit_solution(822677480852057982)
XLA Ops:
  0.6 0.0 copy-start.2
  0.6 0.0 copy-start.3
  0.7 0.0 copy-start.4
  0.7 1.3 multiply_convert_fusion.3
  2.0 0.2 copy.21
  2.1 0.2 copy.20
  2.4 0.8 pad_maximum_fusion.1.dn
  3.2 0.1 multiply_convert_fusion.1
  3.2 0.2 copy.23
  3.4 0.2 copy.22
  3.6 0.1 fusion.5
  3.7 0.9 pad_maximum_fusion.wt
  4.6 171.4 %shard_map.144 = (bf16[2048,768]{1,0:T(8,128)(2,1)}, bf16[2048,768]{1,0:T(8,128)(2,1)}, bf16[352,2048]{1,0:T(8,128)(2,1)}, bf16[352,2048]{1,0:T(8,128)(2,1)}, bf16[64,2048]{1,0:T(8,128)(2,1)}) custom-call(bf16[4,4,64,2048]{3,2,1,0:T(8,128)(2,1)} %bitcast.18, bf16[2,2,128,768]{3,2,1,0:T(8,128)(2,1)} %pad_maximum_fusion.wt, ...), custom_call_target="tpu_custom_call" | custom-call | tf_op jit(solution)/shard_map/pallas_call | solution.py:398
  176.0 2.2 %fusion.9 = (bf16[2048,352]{1,0:T(8,128)(2,1)S(1)}, bf16[2048,352]{1,0:T(8,128)(2,1)S(1)}) fusion(bf16[2048,768]{1,0:T(8,128)(2,1)} %get-tuple-element.12), kind=kLoop, calls=%fused_computation.19 | loop fusion | bytes 5767168 | tf_op jit(solution)/shard_map/slice | solution.py:428
  178.2 1.6 copy.25
  179.8 1.6 copy.24
  181.4 2.2 %fusion.8 = (bf16[2048,352]{1,0:T(8,128)(2,1)S(1)}, bf16[2048,352]{1,0:T(8,128)(2,1)S(1)}) fusion(bf16[2048,768]{1,0:T(8,128)(2,1)} %get-tuple-element.14), kind=kLoop, calls=%fused_computation.18 | loop fusion | bytes 5767168 | tf_op jit(solution)/shard_map/slice | solution.py:429
  183.6 1.6 copy.27
  185.2 1.6 copy.26
  186.8 1.1 copy.31
  187.9 0.8 copy-done
  188.7 1.1 copy.32
  189.8 0.0 copy-done.6
  189.8 0.7 copy.33
  (12 shorter events, 0.1 us)
Async XLA Ops:
  0.6 1.7 copy-start.2
  0.6 1.7 copy-start.3
  0.7 2.5 %copy-start.4 = (f32[128,704]{0,1:T(8,128)S(1)}, f32[128,704]{0,1:T(8,128)}, u32[]{:S(2)}) copy-start(f32[128,704]{0,1:T(8,128)} %param.15) | copy-start | bytes 1081348
  0.7 2.5 %copy-start.5 = (f32[128,704]{0,1:T(8,128)S(1)}, f32[128,704]{0,1:T(8,128)}, u32[]{:S(2)}) copy-start(f32[128,704]{0,1:T(8,128)} %param.16) | copy-start | bytes 1081348
  0.7 2.5 %copy-start.7 = (f32[128]{0:T(128)S(1)}, f32[128]{0:T(128)}, u32[]{:S(2)}) copy-start(f32[128]{0:T(128)} %param.14) | copy-start | bytes 1540
  185.2 1.6 copy-start.1
  186.8 1.9 copy-start
  188.7 1.1 copy-start.6

commit v2 on v1

v2 whole, which is shorter than its diff:
```python
import functools

import jax
import jax.numpy as jnp
from jax import lax
from jax.experimental import pallas as pl
from jax.experimental.pallas import tpu as pltpu
from jax.sharding import PartitionSpec as P

D = 2048
FF = 5632
HB = 352
HP = 384
TOK = 1024
MESH = pl.DeviceIdType.MESH
BF = jnp.bfloat16
F32 = jnp.float32
VMEM_MB = 48
NA = 1152


def rem4(v):
    return lax.rem(v, 4)


def kernel(
    x_hbm, gn1, gt1, ut1, dn1, gn2, gt2, ut2, dn2,
    g1_o, u1_o, d1_o, g2_o, u2_o, d2_o, ps_o,
    nx, ng, xown, mid, raw_w, raw_d, raw_g, wt, dn, gu, dd, act, act2, part, part2,
    r2, ra, rb, tt, acc, sb, q2, qa, qb, qt, ost,
    r2a, raa, rba, ta, acca, sba, rpa, rzb, accb, sbb, r2b, qab, qbb, tb_,
    a_send, w_recv, w_send, d_recv, d_send, d_loc, dp_send, dp_recv,
    rs_send, rs_recv, ag_send, ag_recv, t_send, t_recv, x_sem, i_sem, o_sem,
):
    f = lax.axis_index("fs")
    t = lax.axis_index("tp")
    z = lax.div(f, 4)
    x = lax.rem(f, 4)
    y = lax.div(t, 2)
    core = lax.rem(t, 2)
    sib = (f, 2 * y + 1 - core)
    pending = []

    def send(src, dst, ssem, rsem, dev, cond=None):
        cp = pltpu.make_async_remote_copy(
            src_ref=src, dst_ref=dst, send_sem=ssem, recv_sem=rsem, device_id=dev, device_id_type=MESH
        )
        if cond is None:
            cp.start()
        else:
            pl.when(cond)(cp.start)
        pending.append((cp, cond))

    def drain():
        for cp, cond in pending:
            if cond is None:
                cp.wait_send()
            else:
                pl.when(cond)(cp.wait_send)
        pending.clear()

    def arrived(dst, sem):
        pltpu.make_async_copy(dst, dst, sem).wait()

    barrier = pltpu.get_barrier_semaphore()

    def greet(dev):
        pl.semaphore_signal(barrier, inc=1, device_id=dev, device_id_type=MESH)

    near = [(f, 2 * rem4(y + 1) + core), (f, 2 * rem4(y + 3) + core), sib]
    near += [(4 * z + rem4(x + 1), t), (4 * z + rem4(x + 3), t), (4 * rem4(z + 1) + x, t), (4 * rem4(z + 3) + x, t)]
    for dev in near:
        greet(dev)
    n_self = jnp.int32(0)
    for g, b in ((0, 0), (1, 0), (0, 1), (1, 1)):
        to = (4 * (3 - y if b else y) + 2 * core + g, 2 * x + lax.div(z, 2))
        fro = (4 * (2 * core + g) + y, 2 * (3 - z if b else z) + lax.div(x, 2))
        to_self = jnp.logical_and(to[0] == f, to[1] == t)
        fro_self = jnp.logical_and(fro[0] == f, fro[1] == t)
        pl.when(jnp.logical_not(to_self))(functools.partial(greet, to))
        pl.when(jnp.logical_not(fro_self))(functools.partial(greet, fro))
        n_self = n_self + to_self.astype(jnp.int32) + fro_self.astype(jnp.int32)

    icp = []
    for h, (gn, gt, ut, dw) in enumerate(((gn1, gt1, ut1, dn1), (gn2, gt2, ut2, dn2))):
        for k, (src, dst) in enumerate(
            ((gn, raw_g.at[h]), (gt, raw_w.at[h, 0]), (ut, raw_w.at[h, 1]), (dw, raw_d.at[h]))
        ):
            cp = pltpu.make_async_copy(src, dst, i_sem.at[h, k])
            cp.start()
            icp.append(cp)
    xcp = []
    for r in range(4):
        cp = pltpu.make_async_copy(x_hbm.at[r], nx.at[r], x_sem.at[r])
        cp.start()
        xcp.append(cp)
    own_in = pltpu.make_async_copy(x_hbm.at[z, x], xown, x_sem.at[4])
    own_in.start()

    yp, ym, y2 = rem4(y + 1), rem4(y + 3), rem4(y + 2)

    def tile_id(yy, cc, q):
        return 4 * (2 * cc + q) + yy

    def wv(h, ft):
        return gu.at[h, :, pl.ds(0, HB), pl.ds(pl.multiple_of(ft * 128, 128), 128)]

    a_dt = 2 * x + lax.div(z, 2)

    def stage_a(h):
        for g in range(2):
            src = wt.at[h, :, pl.ds(HB * g, HB), :]
            for slot in ((0,), (1, 2))[h]:
                df = 4 * (3 - y if slot == 2 else y) + 2 * core + g
                same = jnp.logical_and(df == f, a_dt == t)
                send(src, wv(slot, f), a_send.at[slot, g], w_recv.at[slot, f], (df, a_dt), jnp.logical_not(same))

                @pl.when(same)
                def _(src=src, slot=slot):
                    pltpu.make_async_copy(src, wv(slot, f), w_recv.at[slot, f]).start()

    def wsend(h, ft, k, dev):
        send(wv(h, ft), wv(h, ft), w_send.at[h, k], w_recv.at[h, ft], dev)

    up_dev, dn_dev = (f, 2 * yp + core), (f, 2 * ym + core)

    def w_own(h):
        for q in range(2):
            ft = tile_id(y, core, q)
            arrived(wv(h, ft), w_recv.at[h, ft])
            wsend(h, ft, 3 * q, up_dev)
            wsend(h, ft, 3 * q + 1, dn_dev)
            wsend(h, ft, 3 * q + 2, sib)

    def w_fwd(h):
        lo, hi = tile_id(ym, core, 0), tile_id(yp, core, 1)
        arrived(wv(h, lo), w_recv.at[h, lo])
        wsend(h, lo, 6, up_dev)
        arrived(wv(h, hi), w_recv.at[h, hi])
        wsend(h, hi, 7, dn_dev)
        wsend(h, lo, 8, sib)
        wsend(h, hi, 9, sib)

    def w_more(h):
        for k, ft in ((10, tile_id(ym, core, 1)), (11, tile_id(yp, core, 0))):
            arrived(wv(h, ft), w_recv.at[h, ft])
            wsend(h, ft, k, sib)
        for q in range(2):
            ft = tile_id(y2, core, q)
            arrived(wv(h, ft), w_recv.at[h, ft])
            wsend(h, ft, 12 + q, sib)

    def w_end(h):
        for yy in range(4):
            for q in range(2):
                ft = tile_id(yy, 1 - core, q)
                arrived(wv(h, ft), w_recv.at[h, ft])

    def dblk(h, tb, q):
        return dd.at[h, pl.ds(176 * q, 176), pl.ds(pl.multiple_of(tb * 256, 256), 256)]

    def d_local(h):
        return pltpu.make_async_copy(
            dn.at[h], dd.at[h, pl.ds(0, HB), pl.ds(pl.multiple_of(t * 256, 256), 256)], d_loc.at[h]
        )

    def dsend(h, tb, q, k, dev):
        send(dblk(h, tb, q), dblk(h, tb, q), d_send.at[h, k], d_recv.at[h, tb, q], dev)

    def d_own(h):
        if h < 2:
            d_local(h).start()
        else:
            arrived(dcols, dp_recv)
        for q in range(2):
            src = dn.at[h, pl.ds(176 * q, 176), :] if h < 2 else dblk(2, t, q)
            for j, dev in enumerate((up_dev, dn_dev, sib)):
                send(src, dblk(h, t, q), d_send.at[h, 3 * q + j], d_recv.at[h, t, q], dev)

    dcols = dd.at[2, pl.ds(0, HB), pl.ds(pl.multiple_of(t * 256, 256), 256)]

    def d_partner():
        send(dn.at[1], dcols, dp_send, dp_recv, (4 * (3 - z) + x, t))

    def d_fwd(h):
        tm, tp = 2 * ym + core, 2 * yp + core
        arrived(dblk(h, tm, 0), d_recv.at[h, tm, 0])
        dsend(h, tm, 0, 6, up_dev)
        arrived(dblk(h, tp, 1), d_recv.at[h, tp, 1])
        dsend(h, tp, 1, 7, dn_dev)
        dsend(h, tm, 0, 8, sib)
        dsend(h, tp, 1, 9, sib)

    def d_more(h):
        for k, tb, q in ((10, 2 * ym + core, 1), (11, 2 * yp + core, 0), (12, 2 * y2 + core, 0), (13, 2 * y2 + core, 1)):
            arrived(dblk(h, tb, q), d_recv.at[h, tb, q])
            dsend(h, tb, q, k, sib)

    def d_end(h):
        for yy in range(4):
            for q in range(2):
                tb = 2 * yy + 1 - core
                arrived(dblk(h, tb, q), d_recv.at[h, tb, q])
        if h < 2:
            d_local(h).wait()

    def norm_rows(v):
        w = v.astype(F32)
        return (w * lax.rsqrt(jnp.mean(w * w, axis=-1, keepdims=True) + 1e-06)).astype(BF)

    def gate_up(rows, slot):
        w = gu[slot].reshape(2 * HP, D)
        v = lax.dot_general(rows, w, (((1,), (1,)), ((), ())), preferred_element_type=F32)
        gt = v[:, :HP]
        return (gt * jax.nn.sigmoid(gt) * v[:, HP:]).astype(BF)

    def first_act():
        @pl.loop(0, 4)
        def _(r):
            act[r] = gate_up(nx[r].reshape(256, D), 0).reshape(4, 64, HP)

    def second_act():
        @pl.loop(0, 2)
        def _(r):
            rows = ng[r].reshape(256, D)
            for b in range(2):
                act2[r, :, :, HP * b:HP * (b + 1)] = gate_up(rows, 1 + b).reshape(4, 64, HP)

    def colsl(ab):
        return pl.ds(1024 * ab, 1024)

    def pv(h, ab, idx, q):
        if ab == 0:
            return part.at[h, pl.ds(2 * q, 2), idx, :, colsl(0)]
        return part.at[h, idx, pl.ds(2 * q, 2), :, colsl(1)]

    def dev1(ab, step):
        if ab == 0:
            return (4 * z + rem4(x + step + 4), t)
        return (4 * rem4(z + step + 4) + x, t)

    def me1(ab, step):
        return rem4((x if ab == 0 else z) + step + 4)

    def down_chunk(h, ab, idx):
        w = dd[h, :, 1024 * ab:1024 * ab + 1024]
        if ab == 0:
            a = act[:, pl.ds(idx, 1)].reshape(256, HP)
        else:
            a = act[idx].reshape(256, HP)
        v = jnp.dot(a, w, preferred_element_type=F32).astype(BF)
        if ab == 0:
            part[h, :, pl.ds(idx, 1), :, 0:1024] = v.reshape(4, 1, 64, 1024)
        else:
            part[h, idx, :, :, 1024:2048] = v.reshape(4, 64, 1024)

    def s1(h, ab, k, src, dst, step):
        send(src, dst, rs_send.at[h, 0, ab, k], rs_recv.at[h, 0, ab, k], dev1(ab, step))

    def s2(h, ab, k, src, dst, step):
        send(src, dst, rs_send.at[h, 1, ab, k], rs_recv.at[h, 1, ab, k], dev1(1 - ab, step))

    def rs_first(h, between=None):
        for ab in range(2):
            i2 = me1(ab, 2)
            down_chunk(h, ab, i2)
            s1(h, ab, 0, pv(h, ab, i2, 0), r2.at[h, ab, 0], 1)
            s1(h, ab, 1, pv(h, ab, i2, 1), r2.at[h, ab, 1], -1)
        for ab in range(2):
            ip = me1(ab, 1)
            down_chunk(h, ab, ip)
            s1(h, ab, 3, pv(h, ab, ip, 1), ra.at[h, ab, pl.ds(2, 2)], 1)
        for ab in range(2):
            im = me1(ab, -1)
            down_chunk(h, ab, im)
            s1(h, ab, 4, pv(h, ab, im, 0), rb.at[h, ab, pl.ds(0, 2)], -1)
        for ab in range(2):
            down_chunk(h, ab, me1(ab, 0))

    def rs_second(h):
        for ab in range(2):
            arrived(r2.at[h, ab, 0], rs_recv.at[h, 0, ab, 0])
            tt[h, ab, 0] = (r2[h, ab, 0].astype(F32) + pv(h, ab, me1(ab, 1), 0)[...].astype(F32)).astype(BF)
            s1(h, ab, 2, tt.at[h, ab, 0], ra.at[h, ab, pl.ds(0, 2)], 1)
            arrived(r2.at[h, ab, 1], rs_recv.at[h, 0, ab, 1])
            tt[h, ab, 1] = (r2[h, ab, 1].astype(F32) + pv(h, ab, me1(ab, -1), 1)[...].astype(F32)).astype(BF)
            s1(h, ab, 5, tt.at[h, ab, 1], rb.at[h, ab, pl.ds(2, 2)], -1)

    def rs_third(h):
        for ab in range(2):
            for q in range(2):
                sl = pl.ds(2 * q, 2)
                arrived(ra.at[h, ab, sl], rs_recv.at[h, 0, ab, 2 + q])
                arrived(rb.at[h, ab, sl], rs_recv.at[h, 0, ab, 4 + q])
                s = (
                    pv(h, ab, me1(ab, 0), q)[...].astype(F32)
                    + ra[h, ab, 2 * q:2 * q + 2].astype(F32)
                    + rb[h, ab, 2 * q:2 * q + 2].astype(F32)
                )
                acc[ab, 2 * q:2 * q + 2] = s
                sb[h, ab, 2 * q:2 * q + 2] = s.astype(BF)
            i2, ip, im = me1(1 - ab, 2), me1(1 - ab, 1), me1(1 - ab, -1)
            s2(h, ab, 0, sb.at[h, ab, i2, pl.ds(0, 32)], q2.at[h, ab, 0], 1)
            s2(h, ab, 1, sb.at[h, ab, i2, pl.ds(32, 32)], q2.at[h, ab, 1], -1)
            s2(h, ab, 3, sb.at[h, ab, ip, pl.ds(32, 32)], qa.at[h, ab, pl.ds(32, 32)], 1)
            s2(h, ab, 4, sb.at[h, ab, im, pl.ds(0, 32)], qb.at[h, ab, pl.ds(0, 32)], -1)

    def rs_fourth(h):
        for ab in range(2):
            ip, im = me1(1 - ab, 1), me1(1 - ab, -1)
            arrived(q2.at[h, ab, 0], rs_recv.at[h, 1, ab, 0])
            qt[h, ab, 0] = (q2[h, ab, 0].astype(F32) + acc[ab, ip, 0:32]).astype(BF)
            s2(h, ab, 2, qt.at[h, ab, 0], qa.at[h, ab, pl.ds(0, 32)], 1)
            arrived(q2.at[h, ab, 1], rs_recv.at[h, 1, ab, 1])
            qt[h, ab, 1] = (q2[h, ab, 1].astype(F32) + acc[ab, im, 32:64]).astype(BF)
            s2(h, ab, 5, qt.at[h, ab, 1], qb.at[h, ab, pl.ds(32, 32)], -1)
        out = []
        for ab in range(2):
            for q in range(2):
                arrived(qa.at[h, ab, pl.ds(32 * q, 32)], rs_recv.at[h, 1, ab, 2 + q])
                arrived(qb.at[h, ab, pl.ds(32 * q, 32)], rs_recv.at[h, 1, ab, 4 + q])
            out.append(acc[ab, me1(1 - ab, 0)] + qa[h, ab].astype(F32) + qb[h, ab].astype(F32))
        return jnp.concatenate(out, axis=-1)

    zz = lax.rem(z, 2)
    zo = 1 - zz
    pair = (4 * (z + 1 - 2 * zz) + x, t)
    xp, xm, x2 = rem4(x + 1), rem4(x + 3), rem4(x + 2)
    xp_dev, xm_dev = (4 * z + xp, t), (4 * z + xm, t)
    CA, CB = pl.ds(0, NA), pl.ds(NA, D - NA)
    lo, hi = pl.ds(0, 32), pl.ds(32, 32)

    def gv(i, j, cols, rows=slice(None)):
        return ng.at[i, j, rows, cols]

    def gsend(k, ref, dev):
        send(ref, ref, ag_send.at[k], ag_recv.at[k], dev)

    def ag_a():
        gsend(1, gv(zz, x, CA), xp_dev)
        gsend(2, gv(zz, x, CA), xm_dev)
        gsend(7, gv(zz, x, CB), xp_dev)
        gsend(8, gv(zz, x, CB), xm_dev)
        gsend(0, gv(zz, x, CA), pair)
        gsend(9, gv(zz, x, CB), pair)

    def ag_b():
        arrived(gv(zo, x, CA), ag_recv.at[0])
        gsend(3, gv(zo, x, CA), xp_dev)
        gsend(4, gv(zo, x, CA), xm_dev)
        arrived(gv(zz, xm, CA), ag_recv.at[1])
        gsend(5, gv(zz, xm, CA), xp_dev)
        arrived(gv(zz, xm, CB), ag_recv.at[7])
        gsend(10, gv(zz, xm, CB, lo), xp_dev)
        gsend(12, gv(zz, xm, CB), pair)
        arrived(gv(zz, xp, CB), ag_recv.at[8])
        gsend(11, gv(zz, xp, CB, hi), xm_dev)
        gsend(13, gv(zz, xp, CB), pair)
        arrived(gv(zo, xp, CA), ag_recv.at[4])
        gsend(6, gv(zo, xp, CA), xm_dev)
        arrived(gv(zz, x2, CB, lo), ag_recv.at[10])
        arrived(gv(zz, x2, CB, hi), ag_recv.at[11])
        gsend(14, gv(zz, x2, CB), pair)

    def ag_c():
        for k, i, j, c in (
            (2, zz, xp, CA), (3, zo, xm, CA), (5, zz, x2, CA), (6, zo, x2, CA),
            (9, zo, x, CB), (12, zo, xm, CB), (13, zo, xp, CB), (14, zo, x2, CB),
        ):
            arrived(gv(i, j, c), ag_recv.at[k])

    def down2_a(xi):
        w = dd[1:3, :, 0:NA].reshape(2 * HP, NA)
        v = jnp.dot(act2[:, pl.ds(xi, 1)].reshape(128, 2 * HP), w, preferred_element_type=F32).astype(BF)
        part2[:, pl.ds(xi, 1), :, 0:NA] = v.reshape(2, 1, 64, NA)

    def down2_b(zi):
        w = dd[1:3, :, NA:D].reshape(2 * HP, D - NA)
        v = jnp.dot(act2[zi].reshape(256, 2 * HP), w, preferred_element_type=F32).astype(BF)
        part2[zi, :, :, NA:D] = v.reshape(4, 64, D - NA)

    def tsend(k, src, dst, dev):
        send(src, dst, t_send.at[k], t_recv.at[k], dev)

    def rs2():
        down2_b(zo)
        for k, xi in enumerate((x2, xp, xm, x)):
            tsend(k, part2.at[zo, xi, :, CB], rzb.at[xi], pair)
        down2_a(x2)
        tsend(4, part2.at[0, x2, :, CA], r2a.at[0], xp_dev)
        tsend(5, part2.at[1, x2, :, CA], r2a.at[1], xm_dev)
        down2_a(xp)
        tsend(6, part2.at[1, xp, :, CA], raa.at[1], xp_dev)
        down2_a(xm)
        tsend(7, part2.at[0, xm, :, CA], rba.at[0], xm_dev)
        down2_b(zz)
        down2_a(x)

        def fold_b(k, xi):
            arrived(rzb.at[xi], t_recv.at[k])
            s = part2[zz, xi, :, NA:D].astype(F32) + rzb[xi].astype(F32)
            accb[xi] = s
            sbb[xi] = s.astype(BF)

        fold_b(0, x2)
        tsend(8, sbb.at[x2, lo], r2b.at[0], xp_dev)
        tsend(9, sbb.at[x2, hi], r2b.at[1], xm_dev)
        arrived(r2a.at[0], t_recv.at[4])
        ta[0] = (r2a[0].astype(F32) + part2[0, xp, :, 0:NA].astype(F32)).astype(BF)
        tsend(10, ta.at[0], raa.at[0], xp_dev)
        arrived(r2a.at[1], t_recv.at[5])
        ta[1] = (r2a[1].astype(F32) + part2[1, xm, :, 0:NA].astype(F32)).astype(BF)
        tsend(11, ta.at[1], rba.at[1], xm_dev)
        fold_b(1, xp)
        tsend(12, sbb.at[xp, hi], qab.at[hi], xp_dev)
        fold_b(2, xm)
        tsend(13, sbb.at[xm, lo], qbb.at[lo], xm_dev)
        arrived(r2b.at[0], t_recv.at[8])
        tb_[0] = (r2b[0].astype(F32) + accb[xp, 0:32]).astype(BF)
        tsend(14, tb_.at[0], qab.at[lo], xp_dev)
        arrived(r2b.at[1], t_recv.at[9])
        tb_[1] = (r2b[1].astype(F32) + accb[xm, 32:64]).astype(BF)
        tsend(15, tb_.at[1], qbb.at[hi], xm_dev)
        fold_b(3, x)
        arrived(raa.at[1], t_recv.at[6])
        arrived(rba.at[0], t_recv.at[7])
        arrived(raa.at[0], t_recv.at[10])
        arrived(rba.at[1], t_recv.at[11])
        s = part2[zo, x, :, 0:NA].astype(F32) + raa[zo].astype(F32) + rba[zo].astype(F32)
        sba[...] = s.astype(BF)
        tsend(16, sba, rpa, pair)
        own_a = part2[zz, x, :, 0:NA].astype(F32) + raa[zz].astype(F32) + rba[zz].astype(F32)
        arrived(qab.at[hi], t_recv.at[12])
        arrived(qbb.at[lo], t_recv.at[13])
        arrived(qab.at[lo], t_recv.at[14])
        arrived(qbb.at[hi], t_recv.at[15])
        own_b = accb[x] + qab[...].astype(F32) + qbb[...].astype(F32)
        ost[:, NA:D] = (mid[:, NA:D].astype(F32) + 0.5 * own_b).astype(BF)
        arrived(rpa, t_recv.at[16])
        ost[:, 0:NA] = (mid[:, 0:NA].astype(F32) + 0.5 * (own_a + rpa[...].astype(F32))).astype(BF)

    def put(src, dst, k):
        pltpu.make_async_copy(src, dst, o_sem.at[k]).start()

    def put_wait(src, dst, k):
        pltpu.make_async_copy(src, dst, o_sem.at[k]).wait()

    def fold(h):
        for k in range(4):
            icp[4 * h + k].wait()
        for k in range(2):
            wt[h, k] = (raw_g[h] * raw_w[h, k]).astype(BF)
        dn[h] = raw_d[h].astype(BF)

    def norm_first(r):
        xcp[r].wait()
        for k in range(4):
            nx[r, k] = norm_rows(nx[r, k])

    fold(0)
    pl.semaphore_wait(barrier, 15 - n_self)
    stage_a(0)
    d_own(0)
    for s_ in range(3):
        dd[s_, HB:HP, :] = jnp.zeros((HP - HB, D), BF)
        for k in range(2):
            gu[s_, k, HB:HP, :] = jnp.zeros((HP - HB, D), BF)
    for r in range(4):
        norm_first(r)
    fold(1)
    w_own(0)
    d_fwd(0)
    w_fwd(0)
    stage_a(1)
    d_partner()
    d_more(0)
    w_more(0)
    w_end(0)
    put(gu.at[0, 0, pl.ds(0, HB)], g1_o, 0)
    put(gu.at[0, 1, pl.ds(0, HB)], u1_o, 1)

    first_act()
    d_end(0)
    put(dd.at[0, pl.ds(0, HB)], d1_o, 2)
    rs_first(0)
    w_own(1)
    w_own(2)
    rs_second(0)
    d_own(1)
    d_own(2)
    rs_third(0)
    branch = rs_fourth(0)
    own_in.wait()
    m = (xown[...].astype(F32) + 0.5 * branch).astype(BF)
    mid[...] = m
    ng[zz, x] = norm_rows(m)
    ag_a()
    w_fwd(1)
    w_fwd(2)
    ag_b()
    d_fwd(1)
    d_fwd(2)
    for s_ in range(1, 3):
        w_more(s_)
        d_more(s_)
    ag_c()
    for s_ in range(1, 3):
        w_end(s_)
    put(gu.at[1, 0, pl.ds(0, HB)], g2_o, 3)
    put(gu.at[1, 1, pl.ds(0, HB)], u2_o, 4)
    second_act()
    for s_ in range(1, 3):
        d_end(s_)
    put(dd.at[1, pl.ds(0, HB)], d2_o, 5)
    rs2()
    put(ost, ps_o, 6)

    drain()
    put_wait(gu.at[0, 0, pl.ds(0, HB)], g1_o, 0)
    put_wait(gu.at[0, 1, pl.ds(0, HB)], u1_o, 1)
    put_wait(dd.at[0, pl.ds(0, HB)], d1_o, 2)
    put_wait(gu.at[1, 0, pl.ds(0, HB)], g2_o, 3)
    put_wait(gu.at[1, 1, pl.ds(0, HB)], u2_o, 4)
    put_wait(dd.at[1, pl.ds(0, HB)], d2_o, 5)
    put_wait(ost, ps_o, 6)


def copy_out(*refs):
    n = len(refs) // 2
    sems = refs[-1]
    cps = [pltpu.make_async_copy(refs[k], refs[n + k], sems.at[k]) for k in range(n)]
    for cp in cps:
        cp.start()
    for cp in cps:
        cp.wait()


def run(xin, *weights):
    vm = pltpu.VMEM
    dma = pltpu.SemaphoreType.DMA
    w_out = jax.ShapeDtypeStruct((HB, D), BF)
    out_shape = (w_out,) * 6 + (jax.ShapeDtypeStruct((64, D), BF),)
    NB = D - NA
    scratch = [
        vm((4, 4, 64, D), BF), vm((2, 4, 64, D), BF), vm((64, D), BF), vm((64, D), BF),
        vm((2, 2, 2 * HB, 128), F32), vm((2, HB, 256), F32), vm((2, 1, 128), F32),
        vm((2, 2, 2 * HB, 128), BF), vm((2, HB, 256), BF),
        vm((3, 2, HP, D), BF), vm((3, HP, D), BF), vm((4, 4, 64, HP), BF), vm((2, 4, 64, 2 * HP), BF),
        vm((1, 4, 4, 64, D), BF), vm((2, 4, 64, D), BF),
        vm((1, 2, 2, 2, 64, 1024), BF), vm((1, 2, 4, 64, 1024), BF), vm((1, 2, 4, 64, 1024), BF),
        vm((1, 2, 2, 2, 64, 1024), BF), vm((2, 4, 64, 1024), F32), vm((1, 2, 4, 64, 1024), BF),
        vm((1, 2, 2, 32, 1024), BF), vm((1, 2, 64, 1024), BF), vm((1, 2, 64, 1024), BF),
        vm((1, 2, 2, 32, 1024), BF), vm((64, D), BF),
        vm((2, 64, NA), BF), vm((2, 64, NA), BF), vm((2, 64, NA), BF), vm((2, 64, NA), BF),
        vm((2, 64, NA), F32), vm((64, NA), BF), vm((64, NA), BF),
        vm((4, 64, NB), BF), vm((4, 64, NB), F32), vm((4, 64, NB), BF),
        vm((2, 32, NB), BF), vm((64, NB), BF), vm((64, NB), BF), vm((2, 32, NB), BF),
        dma((3, 2)), dma((3, 16)), dma((3, 14)), dma((3, 8, 2)), dma((3, 14)), dma((2,)), dma, dma,
        dma((1, 2, 2, 6)), dma((1, 2, 2, 6)), dma((15,)), dma((15,)), dma((17,)), dma((17,)),
        dma((5,)), dma((2, 4)), dma((7,)),
    ]
    here = [pltpu.with_memory_space_constraint(v, pltpu.HBM) for v in (xin, *weights)]
    outs = pl.pallas_call(
        kernel,
        out_shape=tuple(pltpu.VMEM(o.shape, o.dtype) for o in out_shape),
        in_specs=[pl.BlockSpec(memory_space=pltpu.HBM)] * 9,
        out_specs=tuple(pl.BlockSpec(memory_space=pl.ANY) for _ in range(7)),
        scratch_shapes=scratch,
        compiler_params=pltpu.CompilerParams(
            collective_id=0, has_side_effects=True, vmem_limit_bytes=VMEM_MB * 1024 * 1024
        ),
    )(*here)
    return pl.pallas_call(
        copy_out,
        out_shape=out_shape,
        in_specs=[pl.BlockSpec(memory_space=pl.ANY)] * 7,
        out_specs=tuple(pl.BlockSpec(memory_space=pltpu.HBM) for _ in range(7)),
        scratch_shapes=[dma((7,))],
        compiler_params=pltpu.CompilerParams(vmem_limit_bytes=1024 * 1024),
    )(*outs)


def per_device(
    prompts, gain_first, gate_first, up_first, down_first, gain_second, gate_second, up_second, down_second
):
    xin = prompts.reshape(4, 4, 64, D)
    g1, u1, d1, g2, u2, d2, ps = run(
        xin,
        gain_first.reshape(1, 128), gate_first.T, up_first.T, down_first,
        gain_second.reshape(1, 128), gate_second.T, up_second.T, down_second,
    )
    return g1.T, u1.T, d1, g2.T, u2.T, d2, ps.reshape(1, 64, D)


def solution(mesh):
    w = P("fs", "tp")
    return jax.shard_map(
        per_device,
        mesh=mesh,
        in_specs=(P("tp", None, None), P("fs"), w, w, w, P("fs"), w, w, w),
        out_specs=(
            P(None, "fs"), P(None, "fs"), P("fs", None),
            P(None, "fs"), P(None, "fs"), P("fs", None),
            P("tp", "fs", None),
        ),
        check_vma=False,
    )
```

time: 191 us -> 125 us (0.65)
  Pallas kernels: 171 us -> 124 us
  local copies, waits for them, and re-layouts: 15.1 us -> 0 us
  other arithmetic: 3.18 us -> 0 us
    pallas_call x1 -> x2, Pallas kernels: 171 us -> 124 us  [the longest x1 121 us: run(): pl.pallas_call(kernel, out_shape=tuple((pltpu.VMEM(o.shape, o.dtype) for...]
    unnamed x23 -> x0, local copies, waits for them, and re-layouts: 10 us -> none
    slice x2 -> x0, local copies, waits for them, and re-layouts: 4.4 us -> none  [the longest x1 2.2 us: per_device(): gu1[:, HP:HP + HB]]
where the time goes in v2:
time: 125 us
  Pallas kernels  124 us (99%)
    pallas_call x1, Pallas kernels, run(): pl.pallas_call(kernel, out_shape=tuple((pltpu.VMEM(o.shape, o.dtype) for...  121 us
    pallas_call x1, Pallas kernels, run(): pl.pallas_call(copy_out, out_shape=out_shape, in_specs=[pl.BlockSpec(memo...  3.49 us

profile of v2, /device:TPU:1, one launch (start us, length us, event | category | flops | bytes accessed | tf_op | source)
XLA Modules:
  0.0 125.0 jit_solution(1413119289936961943)
XLA Ops:
  0.6 120.7 %shard_map.144 = (bf16[352,2048]{1,0:T(8,128)(2,1)S(1)}, bf16[352,2048]{1,0:T(8,128)(2,1)S(1)}, bf16[352,2048]{1,0:T(8,128)(2,1)S(1)}, bf16[352,2048]{1,0:T(8,12...) custom-call(bf16[4,4,64,2048]{3,2,1,0:T(8,128)(2,1)} %bitcast.12, ...), custom_call_target="tpu_custom_call" | custom-call | tf_op jit(solution)/shard_map/pallas_call | solution.py:563
  121.3 3.5 %shard_map.145 = (bf16[352,2048]{1,0:T(8,128)(2,1)}, bf16[352,2048]{1,0:T(8,128)(2,1)}, bf16[352,2048]{1,0:T(8,128)(2,1)}, bf16[352,2048]{1,0:T(8,128)(2,1)}, bf...) custom-call(bf16[352,2048]{1,0:T(8,128)(2,1)S(1)} %get-tuple-element.21.refs_0_, ...), custom_call_target="tpu_custom_call" | custom-call | tf_op jit(solution)/shard_map/pallas_call | solution.py:573

commit v3 on v2

--- a/solution.py
+++ b/solution.py
@@ -41,22 +41,24 @@
     sib = (f, 2 * y + 1 - core)
     pending = []
 
-    def send(src, dst, ssem, rsem, dev, cond=None):
-        cp = pltpu.make_async_remote_copy(
+    def remote(src, dst, ssem, rsem, dev):
+        return pltpu.make_async_remote_copy(
             src_ref=src, dst_ref=dst, send_sem=ssem, recv_sem=rsem, device_id=dev, device_id_type=MESH
         )
+
+    def send(src, dst, ssem, rsem, dev, cond=None):
         if cond is None:
-            cp.start()
+            remote(src, dst, ssem, rsem, dev).start()
         else:
-            pl.when(cond)(cp.start)
-        pending.append((cp, cond))
+            pl.when(cond)(lambda: remote(src, dst, ssem, rsem, dev).start())
+        pending.append((src, dst, ssem, rsem, dev, cond))
 
     def drain():
-        for cp, cond in pending:
+        for *args, cond in pending:
             if cond is None:
-                cp.wait_send()
+                remote(*args).wait_send()
             else:
-                pl.when(cond)(cp.wait_send)
+                pl.when(cond)(lambda args=args: remote(*args).wait_send())
         pending.clear()
 
     def arrived(dst, sem):
@@ -72,14 +74,31 @@
     for dev in near:
         greet(dev)
     n_self = jnp.int32(0)
-    for g, b in ((0, 0), (1, 0), (0, 1), (1, 1)):
-        to = (4 * (3 - y if b else y) + 2 * core + g, 2 * x + lax.div(z, 2))
-        fro = (4 * (2 * core + g) + y, 2 * (3 - z if b else z) + lax.div(x, 2))
+    for g in range(2):
+        to = (4 * y + 2 * core + g, 2 * x + lax.div(z, 2))
+        fro = (4 * (2 * core + g) + y, 2 * z + lax.div(x, 2))
         to_self = jnp.logical_and(to[0] == f, to[1] == t)
         fro_self = jnp.logical_and(fro[0] == f, fro[1] == t)
         pl.when(jnp.logical_not(to_self))(functools.partial(greet, to))
         pl.when(jnp.logical_not(fro_self))(functools.partial(greet, fro))
         n_self = n_self + to_self.astype(jnp.int32) + fro_self.astype(jnp.int32)
+
+    par = lax.rem(x + z, 2)
+    for zd in (y, 3 - y):
+        for g in range(2):
+            to = (4 * zd + 2 * core + g, 2 * y + par)
+            to_self = jnp.logical_and(to[0] == f, to[1] == t)
+            pl.when(jnp.logical_not(to_self))(functools.partial(greet, to))
+            n_self = n_self + to_self.astype(jnp.int32)
+    n_fro = jnp.int32(0)
+    for zs in (z, 3 - z):
+        for z2 in range(4):
+            for k in range(2):
+                fr = (4 * z2 + 2 * k + lax.rem(z2 + core, 2), 2 * y + lax.div(x, 2))
+                here = y == zs
+                is_self = jnp.logical_and(fr[0] == f, fr[1] == t)
+                pl.when(jnp.logical_and(here, jnp.logical_not(is_self)))(functools.partial(greet, fr))
+                n_fro = n_fro + jnp.logical_and(here, jnp.logical_not(is_self)).astype(jnp.int32)
 
     icp = []
     for h, (gn, gt, ut, dw) in enumerate(((gn1, gt1, ut1, dn1), (gn2, gt2, ut2, dn2))):
@@ -107,17 +126,52 @@
 
     a_dt = 2 * x + lax.div(z, 2)
 
-    def stage_a(h):
+    def tile_to(h, g, slot, dev):
+        src = wt.at[h, :, pl.ds(HB * g, HB), :]
+        same = jnp.logical_and(dev[0] == f, dev[1] == t)
+        send(src, wv(slot, f), a_send.at[slot, g], w_recv.at[slot, f], dev, jnp.logical_not(same))
+
+        @pl.when(same)
+        def _():
+            pltpu.make_async_copy(src, wv(slot, f), w_recv.at[slot, f]).start()
+
+    def stage_a():
         for g in range(2):
-            src = wt.at[h, :, pl.ds(HB * g, HB), :]
-            for slot in ((0,), (1, 2))[h]:
-                df = 4 * (3 - y if slot == 2 else y) + 2 * core + g
-                same = jnp.logical_and(df == f, a_dt == t)
-                send(src, wv(slot, f), a_send.at[slot, g], w_recv.at[slot, f], (df, a_dt), jnp.logical_not(same))
-
-                @pl.when(same)
-                def _(src=src, slot=slot):
-                    pltpu.make_async_copy(src, wv(slot, f), w_recv.at[slot, f]).start()
+            tile_to(0, g, 0, (4 * y + 2 * core + g, a_dt))
+
+    def stage_a2():
+        for g in range(2):
+            for slot, zd in ((1, y), (2, 3 - y)):
+                tile_to(1, g, slot, (4 * zd + 2 * core + g, 2 * y + par))
+
+    dist = {}
+    for slot, y0 in ((1, z), (2, 3 - z)):
+        dist[slot] = rem4(jnp.where(core == 0, y - y0, y0 - y) + 4)
+    nxt = (f, 2 * rem4(y + 1 + 2 * core) + core)
+
+    def hop(d, batch):
+        for slot in (1, 2):
+            def go(slot=slot):
+                for i in range(4 * batch, 4 * batch + 4):
+                    z2, k = i // 2, i % 2
+                    ft = 4 * z2 + 2 * k + lax.rem(z2 + core, 2)
+                    tile = wv(slot, ft)
+                    arrived(tile, w_recv.at[slot, ft])
+                    if d < 3:
+                        remote(tile, tile, w_send.at[slot, i], w_recv.at[slot, ft], nxt).start()
+                    remote(tile, tile, w_send.at[slot, 8 + i], w_recv.at[slot, ft], sib).start()
+            pl.when(dist[slot] == d)(go)
+
+    def hop_end():
+        for slot in (1, 2):
+            for i in range(8):
+                z2, k = i // 2, i % 2
+                ft = 4 * z2 + 2 * k + lax.rem(z2 + core, 2)
+                tile = wv(slot, ft)
+                pending.append((tile, tile, w_send.at[slot, i], w_recv.at[slot, ft], nxt, dist[slot] < 3))
+                pending.append((tile, tile, w_send.at[slot, 8 + i], w_recv.at[slot, ft], sib, None))
+                fo = 4 * z2 + 2 * k + lax.rem(z2 + 1 - core, 2)
+                arrived(wv(slot, fo), w_recv.at[slot, fo])
 
     def wsend(h, ft, k, dev):
         send(wv(h, ft), wv(h, ft), w_send.at[h, k], w_recv.at[h, ft], dev)
@@ -214,25 +268,25 @@
         gt = v[:, :HP]
         return (gt * jax.nn.sigmoid(gt) * v[:, HP:]).astype(BF)
 
-    def first_act():
-        @pl.loop(0, 4)
-        def _(r):
-            act[r] = gate_up(nx[r].reshape(256, D), 0).reshape(4, 64, HP)
-
-    def second_act():
-        @pl.loop(0, 2)
-        def _(r):
-            rows = ng[r].reshape(256, D)
-            for b in range(2):
-                act2[r, :, :, HP * b:HP * (b + 1)] = gate_up(rows, 1 + b).reshape(4, 64, HP)
-
-    def colsl(ab):
-        return pl.ds(1024 * ab, 1024)
-
-    def pv(h, ab, idx, q):
+    def act_row(zi):
+        act[zi] = gate_up(nx[zi].reshape(256, D), 0).reshape(4, 64, HP)
+
+    def act_col(xi):
+        rows = nx[:, pl.ds(xi, 1)].reshape(256, D)
+        act[:, pl.ds(xi, 1)] = gate_up(rows, 0).reshape(4, 1, 64, HP)
+
+    def act2_row(r):
+        rows = ng[r].reshape(256, D)
+        for b in range(2):
+            act2[r, :, :, HP * b:HP * (b + 1)] = gate_up(rows, 1 + b).reshape(4, 64, HP)
+
+    OFF = (2, 3, 1, 0)
+
+    def pv(ab, i, o):
+        j = rem4((z if ab == 0 else x) + o)
         if ab == 0:
-            return part.at[h, pl.ds(2 * q, 2), idx, :, colsl(0)]
-        return part.at[h, idx, pl.ds(2 * q, 2), :, colsl(1)]
+            return part.at[0, j, i, :, pl.ds(0, 1024)]
+        return part.at[0, i, j, :, pl.ds(1024, 1024)]
 
     def dev1(ab, step):
         if ab == 0:
@@ -242,85 +296,72 @@
     def me1(ab, step):
         return rem4((x if ab == 0 else z) + step + 4)
 
-    def down_chunk(h, ab, idx):
-        w = dd[h, :, 1024 * ab:1024 * ab + 1024]
+    def down_chunk(ab, step):
+        idx = me1(ab, step)
+        w = dd[0, :, 1024 * ab:1024 * ab + 1024]
         if ab == 0:
             a = act[:, pl.ds(idx, 1)].reshape(256, HP)
         else:
             a = act[idx].reshape(256, HP)
         v = jnp.dot(a, w, preferred_element_type=F32).astype(BF)
         if ab == 0:
-            part[h, :, pl.ds(idx, 1), :, 0:1024] = v.reshape(4, 1, 64, 1024)
+            part[0, :, pl.ds(idx, 1), :, 0:1024] = v.reshape(4, 1, 64, 1024)
         else:
-            part[h, idx, :, :, 1024:2048] = v.reshape(4, 64, 1024)
-
-    def s1(h, ab, k, src, dst, step):
-        send(src, dst, rs_send.at[h, 0, ab, k], rs_recv.at[h, 0, ab, k], dev1(ab, step))
-
-    def s2(h, ab, k, src, dst, step):
-        send(src, dst, rs_send.at[h, 1, ab, k], rs_recv.at[h, 1, ab, k], dev1(1 - ab, step))
-
-    def rs_first(h, between=None):
-        for ab in range(2):
-            i2 = me1(ab, 2)
-            down_chunk(h, ab, i2)
-            s1(h, ab, 0, pv(h, ab, i2, 0), r2.at[h, ab, 0], 1)
-            s1(h, ab, 1, pv(h, ab, i2, 1), r2.at[h, ab, 1], -1)
-        for ab in range(2):
-            ip = me1(ab, 1)
-            down_chunk(h, ab, ip)
-            s1(h, ab, 3, pv(h, ab, ip, 1), ra.at[h, ab, pl.ds(2, 2)], 1)
-        for ab in range(2):
-            im = me1(ab, -1)
-            down_chunk(h, ab, im)
-            s1(h, ab, 4, pv(h, ab, im, 0), rb.at[h, ab, pl.ds(0, 2)], -1)
-        for ab in range(2):
-            down_chunk(h, ab, me1(ab, 0))
-
-    def rs_second(h):
-        for ab in range(2):
-            arrived(r2.at[h, ab, 0], rs_recv.at[h, 0, ab, 0])
-            tt[h, ab, 0] = (r2[h, ab, 0].astype(F32) + pv(h, ab, me1(ab, 1), 0)[...].astype(F32)).astype(BF)
-            s1(h, ab, 2, tt.at[h, ab, 0], ra.at[h, ab, pl.ds(0, 2)], 1)
-            arrived(r2.at[h, ab, 1], rs_recv.at[h, 0, ab, 1])
-            tt[h, ab, 1] = (r2[h, ab, 1].astype(F32) + pv(h, ab, me1(ab, -1), 1)[...].astype(F32)).astype(BF)
-            s1(h, ab, 5, tt.at[h, ab, 1], rb.at[h, ab, pl.ds(2, 2)], -1)
-
-    def rs_third(h):
-        for ab in range(2):
-            for q in range(2):
-                sl = pl.ds(2 * q, 2)
-                arrived(ra.at[h, ab, sl], rs_recv.at[h, 0, ab, 2 + q])
-                arrived(rb.at[h, ab, sl], rs_recv.at[h, 0, ab, 4 + q])
-                s = (
-                    pv(h, ab, me1(ab, 0), q)[...].astype(F32)
-                    + ra[h, ab, 2 * q:2 * q + 2].astype(F32)
-                    + rb[h, ab, 2 * q:2 * q + 2].astype(F32)
-                )
-                acc[ab, 2 * q:2 * q + 2] = s
-                sb[h, ab, 2 * q:2 * q + 2] = s.astype(BF)
-            i2, ip, im = me1(1 - ab, 2), me1(1 - ab, 1), me1(1 - ab, -1)
-            s2(h, ab, 0, sb.at[h, ab, i2, pl.ds(0, 32)], q2.at[h, ab, 0], 1)
-            s2(h, ab, 1, sb.at[h, ab, i2, pl.ds(32, 32)], q2.at[h, ab, 1], -1)
-            s2(h, ab, 3, sb.at[h, ab, ip, pl.ds(32, 32)], qa.at[h, ab, pl.ds(32, 32)], 1)
-            s2(h, ab, 4, sb.at[h, ab, im, pl.ds(0, 32)], qb.at[h, ab, pl.ds(0, 32)], -1)
-
-    def rs_fourth(h):
-        for ab in range(2):
-            ip, im = me1(1 - ab, 1), me1(1 - ab, -1)
-            arrived(q2.at[h, ab, 0], rs_recv.at[h, 1, ab, 0])
-            qt[h, ab, 0] = (q2[h, ab, 0].astype(F32) + acc[ab, ip, 0:32]).astype(BF)
-            s2(h, ab, 2, qt.at[h, ab, 0], qa.at[h, ab, pl.ds(0, 32)], 1)
-            arrived(q2.at[h, ab, 1], rs_recv.at[h, 1, ab, 1])
-            qt[h, ab, 1] = (q2[h, ab, 1].astype(F32) + acc[ab, im, 32:64]).astype(BF)
-            s2(h, ab, 5, qt.at[h, ab, 1], qb.at[h, ab, pl.ds(32, 32)], -1)
-        out = []
-        for ab in range(2):
-            for q in range(2):
-                arrived(qa.at[h, ab, pl.ds(32 * q, 32)], rs_recv.at[h, 1, ab, 2 + q])
-                arrived(qb.at[h, ab, pl.ds(32 * q, 32)], rs_recv.at[h, 1, ab, 4 + q])
-            out.append(acc[ab, me1(1 - ab, 0)] + qa[h, ab].astype(F32) + qb[h, ab].astype(F32))
-        return jnp.concatenate(out, axis=-1)
+            part[0, idx, :, :, 1024:2048] = v.reshape(4, 64, 1024)
+
+    def s1(ab, k, src, dst, dev):
+        send(src, dst, rs_send.at[ab, k], rs_recv.at[ab, k], dev)
+
+    def rs_away(ab):
+        for o in OFF:
+            s1(ab, o, pv(ab, me1(ab, 2), o), r2.at[ab, o], dev1(ab, 1 if o in (2, 1) else -1))
+
+    def rs_direct(ab, o):
+        if o in (2, 1):
+            s1(ab, 8 + o, pv(ab, me1(ab, -1), o), rb.at[ab, o], dev1(ab, -1))
+        else:
+            s1(ab, 8 + o, pv(ab, me1(ab, 1), o), ra.at[ab, o], dev1(ab, 1))
+
+    def rs_turn(ab, o):
+        arrived(r2.at[ab, o], rs_recv.at[ab, o])
+        step = 1 if o in (2, 1) else -1
+        tt[ab, o] = (r2[ab, o].astype(F32) + pv(ab, me1(ab, step), o)[...].astype(F32)).astype(BF)
+        s1(ab, 4 + o, tt.at[ab, o], (ra if step == 1 else rb).at[ab, o], dev1(ab, step))
+
+    def rs_fin(ab, o):
+        ka, kb = (4 + o, 8 + o) if o in (2, 1) else (8 + o, 4 + o)
+        arrived(ra.at[ab, o], rs_recv.at[ab, ka])
+        arrived(rb.at[ab, o], rs_recv.at[ab, kb])
+        s = pv(ab, me1(ab, 0), o)[...].astype(F32) + ra[ab, o].astype(F32) + rb[ab, o].astype(F32)
+        acc[ab, o] = s
+        up2, dn2_ = dev1(1 - ab, 1), dev1(1 - ab, -1)
+        lo, hi = pl.ds(0, 32), pl.ds(32, 32)
+        if o != 0:
+            sb[ab, o] = s.astype(BF)
+        if o == 2:
+            s1(ab, 12, sb.at[ab, o, lo], q2.at[ab, 0], up2)
+            s1(ab, 13, sb.at[ab, o, hi], q2.at[ab, 1], dn2_)
+        if o == 1:
+            s1(ab, 15, sb.at[ab, o, hi], qa.at[ab, hi], up2)
+        if o == 3:
+            s1(ab, 16, sb.at[ab, o, lo], qb.at[ab, lo], dn2_)
+
+    def rs_turn2(ab, o):
+        if o == 1:
+            arrived(q2.at[ab, 0], rs_recv.at[ab, 12])
+            qt[ab, 0] = (q2[ab, 0].astype(F32) + acc[ab, 1, 0:32]).astype(BF)
+            s1(ab, 14, qt.at[ab, 0], qa.at[ab, pl.ds(0, 32)], dev1(1 - ab, 1))
+        else:
+            arrived(q2.at[ab, 1], rs_recv.at[ab, 13])
+            qt[ab, 1] = (q2[ab, 1].astype(F32) + acc[ab, 3, 32:64]).astype(BF)
+            s1(ab, 17, qt.at[ab, 1], qb.at[ab, pl.ds(32, 32)], dev1(1 - ab, -1))
+
+    def rs_out(ab):
+        arrived(qa.at[ab, pl.ds(32, 32)], rs_recv.at[ab, 15])
+        arrived(qb.at[ab, pl.ds(0, 32)], rs_recv.at[ab, 16])
+        arrived(qa.at[ab, pl.ds(0, 32)], rs_recv.at[ab, 14])
+        arrived(qb.at[ab, pl.ds(32, 32)], rs_recv.at[ab, 17])
+        return acc[ab, 0] + qa[ab].astype(F32) + qb[ab].astype(F32)
 
     zz = lax.rem(z, 2)
     zo = 1 - zz
@@ -362,9 +403,13 @@
         arrived(gv(zz, x2, CB, hi), ag_recv.at[11])
         gsend(14, gv(zz, x2, CB), pair)
 
-    def ag_c():
+    def ag_own_row():
+        for k, j, c in ((2, xp, CA), (5, x2, CA)):
+            arrived(gv(zz, j, c), ag_recv.at[k])
+
+    def ag_other_row():
         for k, i, j, c in (
-            (2, zz, xp, CA), (3, zo, xm, CA), (5, zz, x2, CA), (6, zo, x2, CA),
+            (3, zo, xm, CA), (6, zo, x2, CA),
             (9, zo, x, CB), (12, zo, xm, CB), (13, zo, xp, CB), (14, zo, x2, CB),
         ):
             arrived(gv(i, j, c), ag_recv.at[k])
@@ -387,12 +432,12 @@
         for k, xi in enumerate((x2, xp, xm, x)):
             tsend(k, part2.at[zo, xi, :, CB], rzb.at[xi], pair)
         down2_a(x2)
-        tsend(4, part2.at[0, x2, :, CA], r2a.at[0], xp_dev)
-        tsend(5, part2.at[1, x2, :, CA], r2a.at[1], xm_dev)
+        tsend(4, part2.at[zo, x2, :, CA], r2a.at[0], xp_dev)
+        tsend(5, part2.at[zz, x2, :, CA], r2a.at[1], xm_dev)
+        down2_a(xm)
+        tsend(7, part2.at[zo, xm, :, CA], rba.at[0], xm_dev)
         down2_a(xp)
-        tsend(6, part2.at[1, xp, :, CA], raa.at[1], xp_dev)
-        down2_a(xm)
-        tsend(7, part2.at[0, xm, :, CA], rba.at[0], xm_dev)
+        tsend(6, part2.at[zz, xp, :, CA], raa.at[1], xp_dev)
         down2_b(zz)
         down2_a(x)
 
@@ -406,15 +451,20 @@
         tsend(8, sbb.at[x2, lo], r2b.at[0], xp_dev)
         tsend(9, sbb.at[x2, hi], r2b.at[1], xm_dev)
         arrived(r2a.at[0], t_recv.at[4])
-        ta[0] = (r2a[0].astype(F32) + part2[0, xp, :, 0:NA].astype(F32)).astype(BF)
+        ta[0] = (r2a[0].astype(F32) + part2[zo, xp, :, 0:NA].astype(F32)).astype(BF)
         tsend(10, ta.at[0], raa.at[0], xp_dev)
         arrived(r2a.at[1], t_recv.at[5])
-        ta[1] = (r2a[1].astype(F32) + part2[1, xm, :, 0:NA].astype(F32)).astype(BF)
+        ta[1] = (r2a[1].astype(F32) + part2[zz, xm, :, 0:NA].astype(F32)).astype(BF)
         tsend(11, ta.at[1], rba.at[1], xm_dev)
         fold_b(1, xp)
         tsend(12, sbb.at[xp, hi], qab.at[hi], xp_dev)
         fold_b(2, xm)
         tsend(13, sbb.at[xm, lo], qbb.at[lo], xm_dev)
+        arrived(rba.at[0], t_recv.at[7])
+        arrived(raa.at[0], t_recv.at[10])
+        s = part2[zo, x, :, 0:NA].astype(F32) + raa[0].astype(F32) + rba[0].astype(F32)
+        sba[...] = s.astype(BF)
+        tsend(16, sba, rpa, pair)
         arrived(r2b.at[0], t_recv.at[8])
         tb_[0] = (r2b[0].astype(F32) + accb[xp, 0:32]).astype(BF)
         tsend(14, tb_.at[0], qab.at[lo], xp_dev)
@@ -423,13 +473,8 @@
         tsend(15, tb_.at[1], qbb.at[hi], xm_dev)
         fold_b(3, x)
         arrived(raa.at[1], t_recv.at[6])
-        arrived(rba.at[0], t_recv.at[7])
-        arrived(raa.at[0], t_recv.at[10])
         arrived(rba.at[1], t_recv.at[11])
-        s = part2[zo, x, :, 0:NA].astype(F32) + raa[zo].astype(F32) + rba[zo].astype(F32)
-        sba[...] = s.astype(BF)
-        tsend(16, sba, rpa, pair)
-        own_a = part2[zz, x, :, 0:NA].astype(F32) + raa[zz].astype(F32) + rba[zz].astype(F32)
+        own_a = part2[zz, x, :, 0:NA].astype(F32) + raa[1].astype(F32) + rba[1].astype(F32)
         arrived(qab.at[hi], t_recv.at[12])
         arrived(qbb.at[lo], t_recv.at[13])
         arrived(qab.at[lo], t_recv.at[14])
@@ -458,9 +503,8 @@
             nx[r, k] = norm_rows(nx[r, k])
 
     fold(0)
-    pl.semaphore_wait(barrier, 15 - n_self)
-    stage_a(0)
-    d_own(0)
+    pl.semaphore_wait(barrier, 15 - n_self + n_fro)
+    stage_a()
     for s_ in range(3):
         dd[s_, HB:HP, :] = jnp.zeros((HP - HB, D), BF)
         for k in range(2):
@@ -469,49 +513,89 @@
         norm_first(r)
     fold(1)
     w_own(0)
-    d_fwd(0)
+    stage_a2()
+    d_partner()
     w_fwd(0)
-    stage_a(1)
-    d_partner()
-    d_more(0)
+    d_own(0)
     w_more(0)
     w_end(0)
     put(gu.at[0, 0, pl.ds(0, HB)], g1_o, 0)
     put(gu.at[0, 1, pl.ds(0, HB)], u1_o, 1)
-
-    first_act()
+    act_col(me1(0, 2))
+    d_fwd(0)
+    act_row(me1(1, 2))
+    d_more(0)
     d_end(0)
+    down_chunk(0, 2)
+    rs_away(0)
+    down_chunk(1, 2)
+    rs_away(1)
     put(dd.at[0, pl.ds(0, HB)], d1_o, 2)
-    rs_first(0)
-    w_own(1)
-    w_own(2)
-    rs_second(0)
+    hop(0, 0)
+    hop(0, 1)
+    act_row(me1(1, -1))
+    down_chunk(1, -1)
+    rs_direct(1, 2)
+    act_row(me1(1, 1))
+    down_chunk(1, 1)
+    rs_direct(1, 3)
+    act_row(me1(1, 0))
+    down_chunk(0, -1)
+    rs_direct(0, 2)
+    down_chunk(0, 1)
+    rs_direct(0, 3)
+    for o in (2, 3):
+        for ab in range(2):
+            rs_turn(ab, o)
+    for o in (1, 0):
+        for ab in range(2):
+            rs_direct(ab, o)
+    for ab in range(2):
+        down_chunk(ab, 0)
     d_own(1)
     d_own(2)
-    rs_third(0)
-    branch = rs_fourth(0)
+    for o in (1, 0):
+        for ab in range(2):
+            rs_turn(ab, o)
+    hop(1, 0)
+    for ab in range(2):
+        rs_fin(ab, 2)
+    for ab in range(2):
+        rs_fin(ab, 3)
+    hop(1, 1)
+    for ab in range(2):
+        rs_turn2(ab, 3)
+    for ab in range(2):
+        rs_fin(ab, 1)
+    for ab in range(2):
+        rs_turn2(ab, 1)
+    for ab in range(2):
+        rs_fin(ab, 0)
+    hop(2, 0)
+    branch = jnp.concatenate([rs_out(0), rs_out(1)], axis=-1)
     own_in.wait()
     m = (xown[...].astype(F32) + 0.5 * branch).astype(BF)
     mid[...] = m
     ng[zz, x] = norm_rows(m)
     ag_a()
-    w_fwd(1)
-    w_fwd(2)
-    ag_b()
+    hop(2, 1)
     d_fwd(1)
     d_fwd(2)
-    for s_ in range(1, 3):
-        w_more(s_)
-        d_more(s_)
-    ag_c()
-    for s_ in range(1, 3):
-        w_end(s_)
+    ag_b()
+    hop(3, 0)
+    d_more(1)
+    d_more(2)
+    hop(3, 1)
+    hop_end()
     put(gu.at[1, 0, pl.ds(0, HB)], g2_o, 3)
     put(gu.at[1, 1, pl.ds(0, HB)], u2_o, 4)
-    second_act()
+    ag_own_row()
+    act2_row(zz)
     for s_ in range(1, 3):
         d_end(s_)
     put(dd.at[1, pl.ds(0, HB)], d2_o, 5)
+    ag_other_row()
+    act2_row(zo)
     rs2()
     put(ost, ps_o, 6)
 
@@ -547,16 +631,16 @@
         vm((2, 2, 2 * HB, 128), BF), vm((2, HB, 256), BF),
         vm((3, 2, HP, D), BF), vm((3, HP, D), BF), vm((4, 4, 64, HP), BF), vm((2, 4, 64, 2 * HP), BF),
         vm((1, 4, 4, 64, D), BF), vm((2, 4, 64, D), BF),
-        vm((1, 2, 2, 2, 64, 1024), BF), vm((1, 2, 4, 64, 1024), BF), vm((1, 2, 4, 64, 1024), BF),
-        vm((1, 2, 2, 2, 64, 1024), BF), vm((2, 4, 64, 1024), F32), vm((1, 2, 4, 64, 1024), BF),
-        vm((1, 2, 2, 32, 1024), BF), vm((1, 2, 64, 1024), BF), vm((1, 2, 64, 1024), BF),
-        vm((1, 2, 2, 32, 1024), BF), vm((64, D), BF),
+        vm((2, 4, 64, 1024), BF), vm((2, 4, 64, 1024), BF), vm((2, 4, 64, 1024), BF),
+        vm((2, 4, 64, 1024), BF), vm((2, 4, 64, 1024), F32), vm((2, 4, 64, 1024), BF),
+        vm((2, 2, 32, 1024), BF), vm((2, 64, 1024), BF), vm((2, 64, 1024), BF),
+        vm((2, 2, 32, 1024), BF), vm((64, D), BF),
         vm((2, 64, NA), BF), vm((2, 64, NA), BF), vm((2, 64, NA), BF), vm((2, 64, NA), BF),
         vm((2, 64, NA), F32), vm((64, NA), BF), vm((64, NA), BF),
         vm((4, 64, NB), BF), vm((4, 64, NB), F32), vm((4, 64, NB), BF),
         vm((2, 32, NB), BF), vm((64, NB), BF), vm((64, NB), BF), vm((2, 32, NB), BF),
-        dma((3, 2)), dma((3, 16)), dma((3, 14)), dma((3, 8, 2)), dma((3, 14)), dma((2,)), dma, dma,
-        dma((1, 2, 2, 6)), dma((1, 2, 2, 6)), dma((15,)), dma((15,)), dma((17,)), dma((17,)),
+        dma((3, 2)), dma((3, 16)), dma((3, 16)), dma((3, 8, 2)), dma((3, 14)), dma((2,)), dma, dma,
+        dma((2, 18)), dma((2, 18)), dma((15,)), dma((15,)), dma((17,)), dma((17,)),
         dma((5,)), dma((2, 4)), dma((7,)),
     ]
     here = [pltpu.with_memory_space_constraint(v, pltpu.HBM) for v in (xin, *weights)]

time: 125 us -> 123 us (0.984)
  Pallas kernels: 124 us -> 122 us
    pallas_call x1, Pallas kernels: 121 us -> 119 us  [run(): pl.pallas_call(kernel, out_shape=tuple((pltpu.VMEM(o.shape, o.dtype) for...]
where the time goes in v3:
time: 123 us
  Pallas kernels  122 us (99%)
    pallas_call x1, Pallas kernels, run(): pl.pallas_call(kernel, out_shape=tuple((pltpu.VMEM(o.shape, o.dtype) for...  119 us
    pallas_call x1, Pallas kernels, run(): pl.pallas_call(copy_out, out_shape=out_shape, in_specs=[pl.BlockSpec(memo...  3.49 us

profile of v3, /device:TPU:1, one launch (start us, length us, event | category | flops | bytes accessed | tf_op | source)
XLA Modules:
  0.0 123.3 jit_solution(17384917568509618148)
XLA Ops:
  0.6 119.0 %shard_map.144 = (bf16[352,2048]{1,0:T(8,128)(2,1)S(1)}, bf16[352,2048]{1,0:T(8,128)(2,1)S(1)}, bf16[352,2048]{1,0:T(8,128)(2,1)S(1)}, bf16[352,2048]{1,0:T(8,12...) custom-call(bf16[4,4,64,2048]{3,2,1,0:T(8,128)(2,1)} %bitcast.12, ...), custom_call_target="tpu_custom_call" | custom-call | tf_op jit(solution)/shard_map/pallas_call | solution.py:647
  119.6 3.5 %shard_map.145 = (bf16[352,2048]{1,0:T(8,128)(2,1)}, bf16[352,2048]{1,0:T(8,128)(2,1)}, bf16[352,2048]{1,0:T(8,128)(2,1)}, bf16[352,2048]{1,0:T(8,128)(2,1)}, bf...) custom-call(bf16[352,2048]{1,0:T(8,128)(2,1)S(1)} %get-tuple-element.21.refs_0_, ...), custom_call_target="tpu_custom_call" | custom-call | tf_op jit(solution)/shard_map/pallas_call | solution.py:657

commit v4 on v2

v4 whole, which is shorter than its diff:
```python
import functools

import jax
import jax.numpy as jnp
from jax import lax
from jax.experimental import pallas as pl
from jax.experimental.pallas import tpu as pltpu
from jax.sharding import PartitionSpec as P

D = 2048
FF = 5632
HB = 352
HP = 384
TOK = 1024
MESH = pl.DeviceIdType.MESH
BF = jnp.bfloat16
F32 = jnp.float32
VMEM_MB = 53
POOL = 64


def rem4(v):
    return lax.rem(v, 4)


def kernel(
    x_hbm, gn1, gt1, ut1, dn1, gn2, gt2, ut2, dn2,
    g1_o, u1_o, d1_o, g2_o, u2_o, d2_o, ps_o,
    nx, ng, xown, mid, raw_w, raw_d, raw_g, wt, dn, gu, dd, act, part,
    gates, r2, ra, rb, tt, acc, sb, q2, qa, qb, qt, ost,
    pool, w1_recv, w_recv, w_send, d_recv, d_loc, rs_recv, ag_recv, x_sem, i_sem, o_sem,
):
    f = lax.axis_index("fs")
    t = lax.axis_index("tp")
    z = lax.div(f, 4)
    x = lax.rem(f, 4)
    y = lax.div(t, 2)
    core = lax.rem(t, 2)
    sib = (f, 2 * y + 1 - core)
    pending = []

    def remote(src, dst, ssem, rsem, dev):
        return pltpu.make_async_remote_copy(
            src_ref=src, dst_ref=dst, send_sem=ssem, recv_sem=rsem, device_id=dev, device_id_type=MESH
        )

    taken = []

    def settle(src, dst, ssem, rsem, dev, cond):
        if cond is None:
            remote(src, dst, ssem, rsem, dev).wait_send()
        else:
            pl.when(cond)(lambda: remote(src, dst, ssem, rsem, dev).wait_send())

    def send(src, dst, rsem, dev, cond=None):
        k = len(taken)
        if k >= POOL:
            settle(*taken[k - POOL])
        ssem = pool.at[k % POOL]
        if cond is None:
            remote(src, dst, ssem, rsem, dev).start()
        else:
            pl.when(cond)(lambda: remote(src, dst, ssem, rsem, dev).start())
        taken.append((src, dst, ssem, rsem, dev, cond))

    def drain():
        for item in taken[-POOL:] + pending:
            settle(*item)

    def arrived(dst, sem):
        pltpu.make_async_copy(dst, dst, sem).wait()

    def a_dt(g):
        return 2 * rem4(y + 2 + x - 2 * core - g + 4) + lax.div(z, 2)

    def tile_id(yy, cc, q):
        return 4 * (2 * cc + q) + rem4(yy - z + 2 + x + 4)

    barrier = pltpu.get_barrier_semaphore()

    def greet(dev):
        pl.semaphore_signal(barrier, inc=1, device_id=dev, device_id_type=MESH)

    near = [(f, 2 * rem4(y + 1) + core), (f, 2 * rem4(y + 3) + core), sib]
    near += [(4 * z + rem4(x + 1), t), (4 * z + rem4(x + 3), t), (4 * rem4(z + 1) + x, t), (4 * rem4(z + 3) + x, t)]
    for dev in near:
        greet(dev)
    n_self = jnp.int32(0)
    for g in range(2):
        to = (4 * y + 2 * core + g, a_dt(g))
        fro = (tile_id(y, core, g), 2 * z + lax.div(x, 2))
        to_self = jnp.logical_and(to[0] == f, to[1] == t)
        fro_self = jnp.logical_and(fro[0] == f, fro[1] == t)
        pl.when(jnp.logical_not(to_self))(functools.partial(greet, to))
        pl.when(jnp.logical_not(fro_self))(functools.partial(greet, fro))
        n_self = n_self + to_self.astype(jnp.int32) + fro_self.astype(jnp.int32)

    par = lax.rem(x + z, 2)
    for g in range(2):
        to = (4 * y + 2 * core + g, 2 * y + par)
        to_self = jnp.logical_and(to[0] == f, to[1] == t)
        pl.when(jnp.logical_not(to_self))(functools.partial(greet, to))
        n_self = n_self + to_self.astype(jnp.int32)
    n_fro = jnp.int32(0)
    for z2 in range(4):
        for k in range(2):
            fr = (4 * z2 + 2 * k + lax.rem(z2 + core, 2), 2 * y + lax.div(x, 2))
            is_self = jnp.logical_and(fr[0] == f, fr[1] == t)
            there = jnp.logical_and(y == z, jnp.logical_not(is_self))
            pl.when(there)(functools.partial(greet, fr))
            n_fro = n_fro + there.astype(jnp.int32)

    icp = []
    for h, (gn, gt, ut, dw) in enumerate(((gn1, gt1, ut1, dn1), (gn2, gt2, ut2, dn2))):
        for k, (src, dst) in enumerate(
            ((gn, raw_g.at[h]), (gt, raw_w.at[h, 0]), (ut, raw_w.at[h, 1]), (dw, raw_d.at[h]))
        ):
            cp = pltpu.make_async_copy(src, dst, i_sem.at[h, k])
            cp.start()
            icp.append(cp)
    xcp = []
    for r in range(4):
        cp = pltpu.make_async_copy(x_hbm.at[r], nx.at[r], x_sem.at[r])
        cp.start()
        xcp.append(cp)
    own_in = pltpu.make_async_copy(x_hbm.at[z, x], xown, x_sem.at[4])
    own_in.start()

    yp, ym, y2 = rem4(y + 1), rem4(y + 3), rem4(y + 2)


    def w1(k, ft):
        return gu.at[0, k, pl.ds(0, HB), pl.ds(pl.multiple_of(ft * 128, 128), 128)]

    def stage_a():
        for k in range(2):
            for g in range(2):
                src = wt.at[0, k, pl.ds(HB * g, HB), :]
                dev = (4 * y + 2 * core + g, a_dt(g))
                same = jnp.logical_and(dev[0] == f, dev[1] == t)
                send(src, w1(k, f), w1_recv.at[k, f], dev, jnp.logical_not(same))

                @pl.when(same)
                def _(src=src, k=k):
                    pltpu.make_async_copy(src, w1(k, f), w1_recv.at[k, f]).start()

    def wv(ft):
        return gu.at[1, :, pl.ds(0, HB), pl.ds(pl.multiple_of(ft * 128, 128), 128)]

    def stage_a2():
        for g in range(2):
            src = wt.at[1, :, pl.ds(HB * g, HB), :]
            dev = (4 * y + 2 * core + g, 2 * y + par)
            same = jnp.logical_and(dev[0] == f, dev[1] == t)
            send(src, wv(f), w_recv.at[f], dev, jnp.logical_not(same))

            @pl.when(same)
            def _(src=src):
                pltpu.make_async_copy(src, wv(f), w_recv.at[f]).start()

    nxt = (f, 2 * rem4(y + 1 + 2 * core) + core)
    dist = rem4(jnp.where(core == 0, y - z, z - y) + 4)

    def chain_tile(i, cc):
        z2, k = i // 2, i % 2
        return 4 * z2 + 2 * k + lax.rem(z2 + cc, 2)

    def hop(d, batch):
        @pl.when(dist == d)
        def _():
            for i in range(4 * batch, 4 * batch + 4):
                ft = chain_tile(i, core)
                tile = wv(ft)
                arrived(tile, w_recv.at[ft])
                if d < 3:
                    remote(tile, tile, w_send.at[i], w_recv.at[ft], nxt).start()
                remote(tile, tile, w_send.at[8 + i], w_recv.at[ft], sib).start()

    def hop_end():
        for i in range(8):
            ft = chain_tile(i, core)
            tile = wv(ft)
            pending.append((tile, tile, w_send.at[i], w_recv.at[ft], nxt, dist < 3))
            pending.append((tile, tile, w_send.at[8 + i], w_recv.at[ft], sib, None))
            fo = chain_tile(i, 1 - core)
            arrived(wv(fo), w_recv.at[fo])

    def wsend(k, ft, dev):
        send(w1(k, ft), w1(k, ft), w1_recv.at[k, ft], dev)

    def wgot(k, ft):
        arrived(w1(k, ft), w1_recv.at[k, ft])

    up_dev, dn_dev = (f, 2 * yp + core), (f, 2 * ym + core)

    def w_own():
        for k in range(2):
            for q in range(2):
                ft = tile_id(y, core, q)
                wgot(k, ft)
                for dev in (up_dev, dn_dev, sib):
                    wsend(k, ft, dev)

    def w_fwd(k):
        lo, hi = tile_id(ym, core, 0), tile_id(yp, core, 1)
        wgot(k, lo)
        wsend(k, lo, up_dev)
        wgot(k, hi)
        wsend(k, hi, dn_dev)
        wsend(k, lo, sib)
        wsend(k, hi, sib)

    def w_more(k):
        for ft in (tile_id(ym, core, 1), tile_id(yp, core, 0)):
            wgot(k, ft)
            wsend(k, ft, sib)
        for q in range(2):
            ft = tile_id(y2, core, q)
            wgot(k, ft)
            wsend(k, ft, sib)

    def w_end(k):
        for yy in range(4):
            for q in range(2):
                wgot(k, tile_id(yy, 1 - core, q))

    def dblk(h, tb, q):
        return dd.at[h, pl.ds(176 * q, 176), pl.ds(pl.multiple_of(tb * 256, 256), 256)]

    def d_local(h):
        return pltpu.make_async_copy(
            dn.at[h], dd.at[h, pl.ds(0, HB), pl.ds(pl.multiple_of(t * 256, 256), 256)], d_loc.at[h]
        )

    def dsend(h, tb, q, dev):
        send(dblk(h, tb, q), dblk(h, tb, q), d_recv.at[h, tb, q], dev)

    def d_own(h):
        d_local(h).start()
        for q in range(2):
            src = dn.at[h, pl.ds(176 * q, 176), :]
            for dev in (up_dev, dn_dev, sib):
                send(src, dblk(h, t, q), d_recv.at[h, t, q], dev)

    def d_fwd(h):
        tm, tp = 2 * ym + core, 2 * yp + core
        arrived(dblk(h, tm, 0), d_recv.at[h, tm, 0])
        dsend(h, tm, 0, up_dev)
        arrived(dblk(h, tp, 1), d_recv.at[h, tp, 1])
        dsend(h, tp, 1, dn_dev)
        dsend(h, tm, 0, sib)
        dsend(h, tp, 1, sib)

    def d_more(h):
        for tb, q in ((2 * ym + core, 1), (2 * yp + core, 0), (2 * y2 + core, 0), (2 * y2 + core, 1)):
            arrived(dblk(h, tb, q), d_recv.at[h, tb, q])
            dsend(h, tb, q, sib)

    def d_end(h):
        for yy in range(4):
            for q in range(2):
                tb = 2 * yy + 1 - core
                arrived(dblk(h, tb, q), d_recv.at[h, tb, q])
        d_local(h).wait()

    def norm_rows(v):
        w = v.astype(F32)
        return (w * lax.rsqrt(jnp.mean(w * w, axis=-1, keepdims=True) + 1e-06)).astype(BF)

    def gate_up(rows, slot):
        w = gu[slot].reshape(2 * HP, D)
        v = lax.dot_general(rows, w, (((1,), (1,)), ((), ())), preferred_element_type=F32)
        gt = v[:, :HP]
        return (gt * jax.nn.sigmoid(gt) * v[:, HP:]).astype(BF)

    def nt_dot(rows, w):
        return lax.dot_general(rows, w, (((1,), (1,)), ((), ())), preferred_element_type=F32)

    def gate_row(zi):
        gates[zi] = nt_dot(nx[zi].reshape(256, D), gu[0, 0]).reshape(4, 64, HP)

    def with_gate(gt, rows):
        return (gt * jax.nn.sigmoid(gt) * nt_dot(rows, gu[0, 1])).astype(BF)

    def act_row(h, zi):
        if h == 1:
            act[zi] = gate_up(ng[zi].reshape(256, D), 1).reshape(4, 64, HP)
        else:
            act[zi] = with_gate(gates[zi].reshape(256, HP), nx[zi].reshape(256, D)).reshape(4, 64, HP)

    def act_col(xi):
        rows = nx[:, pl.ds(xi, 1)].reshape(256, D)
        act[:, pl.ds(xi, 1)] = with_gate(gates[:, pl.ds(xi, 1)].reshape(256, HP), rows).reshape(4, 1, 64, HP)

    OFF = (2, 3, 1, 0)

    def pv(h, ab, i, o):
        j = rem4((z if ab == 0 else x) + o)
        if ab == 0:
            return part.at[h, j, i, :, pl.ds(0, 1024)]
        return part.at[h, i, j, :, pl.ds(1024, 1024)]

    def dev1(ab, step):
        if ab == 0:
            return (4 * z + rem4(x + step + 4), t)
        return (4 * rem4(z + step + 4) + x, t)

    def me1(ab, step):
        return rem4((x if ab == 0 else z) + step + 4)

    def down_chunk(h, ab, step):
        idx = me1(ab, step)
        w = dd[h, :, 1024 * ab:1024 * ab + 1024]
        if ab == 0:
            a = act[:, pl.ds(idx, 1)].reshape(256, HP)
        else:
            a = act[idx].reshape(256, HP)
        v = jnp.dot(a, w, preferred_element_type=F32).astype(BF)
        if ab == 0:
            part[h, :, pl.ds(idx, 1), :, 0:1024] = v.reshape(4, 1, 64, 1024)
        else:
            part[h, idx, :, :, 1024:2048] = v.reshape(4, 64, 1024)

    def s1(h, ab, k, src, dst, dev):
        send(src, dst, rs_recv.at[ab, k], dev)

    def rs_away(h, ab):
        for o in OFF:
            s1(h, ab, o, pv(h, ab, me1(ab, 2), o), r2.at[h, ab, o], dev1(ab, 1 if o in (2, 1) else -1))

    def rs_direct(h, ab, o):
        if o in (2, 1):
            s1(h, ab, 8 + o, pv(h, ab, me1(ab, -1), o), rb.at[h, ab, o], dev1(ab, -1))
        else:
            s1(h, ab, 8 + o, pv(h, ab, me1(ab, 1), o), ra.at[h, ab, o], dev1(ab, 1))

    def rs_turn(h, ab, o):
        arrived(r2.at[h, ab, o], rs_recv.at[ab, o])
        step = 1 if o in (2, 1) else -1
        tt[h, ab, o] = (r2[h, ab, o].astype(F32) + pv(h, ab, me1(ab, step), o)[...].astype(F32)).astype(BF)
        s1(h, ab, 4 + o, tt.at[h, ab, o], (ra if step == 1 else rb).at[h, ab, o], dev1(ab, step))

    def rs_fin(h, ab, o):
        ka, kb = (4 + o, 8 + o) if o in (2, 1) else (8 + o, 4 + o)
        arrived(ra.at[h, ab, o], rs_recv.at[ab, ka])
        arrived(rb.at[h, ab, o], rs_recv.at[ab, kb])
        s = pv(h, ab, me1(ab, 0), o)[...].astype(F32) + ra[h, ab, o].astype(F32) + rb[h, ab, o].astype(F32)
        acc[ab, o] = s
        up2, dn2_ = dev1(1 - ab, 1), dev1(1 - ab, -1)
        lo, hi = pl.ds(0, 32), pl.ds(32, 32)
        if o != 0:
            sb[h, ab, o] = s.astype(BF)
        if o == 2:
            s1(h, ab, 12, sb.at[h, ab, o, lo], q2.at[h, ab, 0], up2)
            s1(h, ab, 13, sb.at[h, ab, o, hi], q2.at[h, ab, 1], dn2_)
        if o == 1:
            s1(h, ab, 15, sb.at[h, ab, o, hi], qa.at[h, ab, hi], up2)
        if o == 3:
            s1(h, ab, 16, sb.at[h, ab, o, lo], qb.at[h, ab, lo], dn2_)

    def rs_turn2(h, ab, o):
        if o == 1:
            arrived(q2.at[h, ab, 0], rs_recv.at[ab, 12])
            qt[h, ab, 0] = (q2[h, ab, 0].astype(F32) + acc[ab, 1, 0:32]).astype(BF)
            s1(h, ab, 14, qt.at[h, ab, 0], qa.at[h, ab, pl.ds(0, 32)], dev1(1 - ab, 1))
        else:
            arrived(q2.at[h, ab, 1], rs_recv.at[ab, 13])
            qt[h, ab, 1] = (q2[h, ab, 1].astype(F32) + acc[ab, 3, 32:64]).astype(BF)
            s1(h, ab, 17, qt.at[h, ab, 1], qb.at[h, ab, pl.ds(32, 32)], dev1(1 - ab, -1))

    def rs_out(h, ab):
        arrived(qa.at[h, ab, pl.ds(32, 32)], rs_recv.at[ab, 15])
        arrived(qb.at[h, ab, pl.ds(0, 32)], rs_recv.at[ab, 16])
        arrived(qa.at[h, ab, pl.ds(0, 32)], rs_recv.at[ab, 14])
        arrived(qb.at[h, ab, pl.ds(32, 32)], rs_recv.at[ab, 17])
        return acc[ab, 0] + qa[h, ab].astype(F32) + qb[h, ab].astype(F32)

    def rs_run(h, points):
        def point(k):
            for fn in points.get(k, ()):
                fn()

        down_chunk(h, 0, 2)
        rs_away(h, 0)
        down_chunk(h, 1, 2)
        rs_away(h, 1)
        point(0)
        down_chunk(h, 1, -1)
        rs_direct(h, 1, 2)
        point(1)
        down_chunk(h, 1, 1)
        point(2)
        down_chunk(h, 0, -1)
        rs_direct(h, 0, 2)
        down_chunk(h, 0, 1)
        for ab in (1, 0):
            rs_turn(h, ab, 2)
            rs_direct(h, ab, 3)
            rs_turn(h, ab, 3)
        point(3)
        for ab in (1, 0):
            rs_turn(h, ab, 1)
            rs_direct(h, ab, 1)
        for ab in range(2):
            down_chunk(h, ab, 0)
        for ab in (1, 0):
            rs_fin(h, ab, 2)
        for ab in (1, 0):
            rs_direct(h, ab, 0)
        for ab in (1, 0):
            rs_fin(h, ab, 3)
            rs_turn(h, ab, 0)
        point(4)
        for ab in (1, 0):
            rs_fin(h, ab, 1)
        point(5)
        for ab in (1, 0):
            rs_turn2(h, ab, 3)
            rs_turn2(h, ab, 1)
        for ab in (1, 0):
            rs_fin(h, ab, 0)
        point(6)
        return jnp.concatenate([rs_out(h, 0), rs_out(h, 1)], axis=-1)

    lo_rows, hi_rows = pl.ds(0, 32), pl.ds(32, 32)
    waited = set()

    def gv(ab, i, j, rows=slice(None)):
        zi, xi = (i, j) if ab == 0 else (j, i)
        return ng.at[rem4(z + zi), rem4(x + xi), rows, pl.ds(1024 * ab, 1024)]

    LAND = {
        0: (3, 0), 1: (1, 0), 2: (2, 0, lo_rows), 3: (2, 0, hi_rows),
        4: (0, 3), 5: (1, 3), 6: (2, 3), 7: (3, 3),
        8: (0, 1), 9: (1, 1), 10: (2, 1), 11: (3, 1),
        12: (0, 2), 13: (1, 2), 14: (3, 2), 15: (2, 2),
    }

    def got(ab, *slots):
        for k in slots:
            if (ab, k) not in waited:
                waited.add((ab, k))
                arrived(gv(ab, *LAND[k]), ag_recv.at[ab, k])

    def snd(ab, k, ref, second, step):
        send(ref, ref, ag_recv.at[ab, k], dev1(ab if second else 1 - ab, step))

    def ag_start():
        for ab in range(2):
            own = gv(ab, 0, 0)
            snd(ab, 0, own, False, 1)
            snd(ab, 1, own, False, -1)
            snd(ab, 4, own, True, 1)
            snd(ab, 8, own, True, -1)

    def ag_first():
        for ab in range(2):
            got(ab, 0)
            snd(ab, 2, gv(ab, 3, 0, lo_rows), False, 1)
            got(ab, 1)
            snd(ab, 3, gv(ab, 1, 0, hi_rows), False, -1)
            snd(ab, 5, gv(ab, 1, 0), True, 1)
            snd(ab, 11, gv(ab, 3, 0), True, -1)
            snd(ab, 7, gv(ab, 3, 0), True, 1)
            snd(ab, 9, gv(ab, 1, 0), True, -1)

    def ag_second():
        for ab in range(2):
            got(ab, 4)
            snd(ab, 12, gv(ab, 0, 3), True, 1)
        for ab in range(2):
            got(ab, 2, 3)
            snd(ab, 10, gv(ab, 2, 0), True, -1)
            snd(ab, 6, gv(ab, 2, 0), True, 1)

    def ag_third():
        for ab in range(2):
            got(ab, 5)
            snd(ab, 13, gv(ab, 1, 3), True, 1)
            got(ab, 8, 11)
            snd(ab, 14, gv(ab, 3, 1), True, -1)

    def ag_fourth():
        for ab in range(2):
            got(ab, 9, 10)
            snd(ab, 15, gv(ab, 2, 1), True, -1)

    def ag_row(oz):
        for k, v in LAND.items():
            if v[0] == oz:
                got(0, k)
            if v[1] == oz:
                got(1, k)

    def put(src, dst, k):
        pltpu.make_async_copy(src, dst, o_sem.at[k]).start()

    def put_wait(src, dst, k):
        pltpu.make_async_copy(src, dst, o_sem.at[k]).wait()

    def fold(h):
        for k in range(4):
            icp[4 * h + k].wait()
        for k in range(2):
            wt[h, k] = (raw_g[h] * raw_w[h, k]).astype(BF)
        dn[h] = raw_d[h].astype(BF)

    def norm_first(r):
        xcp[r].wait()
        for k in range(4):
            nx[r, k] = norm_rows(nx[r, k])

    fold(0)
    pl.semaphore_wait(barrier, 13 - n_self + n_fro)
    stage_a()
    d_own(0)
    for s_ in range(2):
        dd[s_, HB:HP, :] = jnp.zeros((HP - HB, D), BF)
        for k in range(2):
            gu[s_, k, HB:HP, :] = jnp.zeros((HP - HB, D), BF)
    for r in range(4):
        norm_first(r)
    fold(1)
    w_own()
    stage_a2()
    w_fwd(0)
    w_fwd(1)
    d_fwd(0)
    w_more(0)
    w_end(0)
    gate_row(0)
    gate_row(1)
    w_more(1)
    gate_row(2)
    gate_row(3)
    w_end(1)
    put(gu.at[0, 0, pl.ds(0, HB)], g1_o, 0)
    put(gu.at[0, 1, pl.ds(0, HB)], u1_o, 1)
    act_col(rem4(x + 2))
    act_row(0, rem4(z + 2))
    d_more(0)
    d_end(0)
    put(dd.at[0, pl.ds(0, HB)], d1_o, 2)
    branch = rs_run(0, {
        0: (lambda: hop(0, 0), lambda: hop(0, 1), lambda: act_row(0, rem4(z + 3))),
        1: (lambda: act_row(0, rem4(z + 1)),),
        2: (lambda: act_row(0, z),),
        3: (lambda: hop(1, 0),),
        4: (lambda: hop(1, 1),),
        5: (lambda: hop(2, 0),),
        6: (lambda: d_own(1),),
    })
    own_in.wait()
    m = (xown[...].astype(F32) + 0.5 * branch).astype(BF)
    mid[...] = m
    ng[z, x] = norm_rows(m)
    ag_start()
    hop(2, 1)
    ag_first()
    ag_second()
    d_fwd(1)
    hop(3, 0)
    ag_third()
    hop(3, 1)
    hop_end()
    ag_row(0)
    act_row(1, z)
    ag_fourth()
    put(gu.at[1, 0, pl.ds(0, HB)], g2_o, 3)
    put(gu.at[1, 1, pl.ds(0, HB)], u2_o, 4)
    for oz in (1, 3):
        ag_row(oz)
        act_row(1, rem4(z + oz))
    d_more(1)
    ag_row(2)
    act_row(1, rem4(z + 2))
    d_end(1)
    put(dd.at[1, pl.ds(0, HB)], d2_o, 5)
    branch = rs_run(1, {})
    ost[...] = (mid[...].astype(F32) + 0.5 * branch).astype(BF)
    put(ost, ps_o, 6)

    drain()
    put_wait(gu.at[0, 0, pl.ds(0, HB)], g1_o, 0)
    put_wait(gu.at[0, 1, pl.ds(0, HB)], u1_o, 1)
    put_wait(dd.at[0, pl.ds(0, HB)], d1_o, 2)
    put_wait(gu.at[1, 0, pl.ds(0, HB)], g2_o, 3)
    put_wait(gu.at[1, 1, pl.ds(0, HB)], u2_o, 4)
    put_wait(dd.at[1, pl.ds(0, HB)], d2_o, 5)
    put_wait(ost, ps_o, 6)


def copy_out(*refs):
    n = len(refs) // 2
    sems = refs[-1]
    cps = [pltpu.make_async_copy(refs[k], refs[n + k], sems.at[k]) for k in range(n)]
    for cp in cps:
        cp.start()
    for cp in cps:
        cp.wait()


def run(xin, *weights):
    vm = pltpu.VMEM
    dma = pltpu.SemaphoreType.DMA
    w_out = jax.ShapeDtypeStruct((HB, D), BF)
    out_shape = (w_out,) * 6 + (jax.ShapeDtypeStruct((64, D), BF),)
    unit = (2, 2, 4, 64, 1024)
    half = (2, 2, 2, 32, 1024)
    one = (2, 2, 64, 1024)
    scratch = [
        vm((4, 4, 64, D), BF), vm((4, 4, 64, D), BF), vm((64, D), BF), vm((64, D), BF),
        vm((2, 2, 2 * HB, 128), F32), vm((2, HB, 256), F32), vm((2, 1, 128), F32),
        vm((2, 2, 2 * HB, 128), BF), vm((2, HB, 256), BF),
        vm((2, 2, HP, D), BF), vm((2, HP, D), BF), vm((4, 4, 64, HP), BF), vm((2, 4, 4, 64, D), BF),
        vm((4, 4, 64, HP), F32),
        vm(unit, BF), vm(unit, BF), vm(unit, BF), vm(unit, BF), vm((2, 4, 64, 1024), F32), vm(unit, BF),
        vm(half, BF), vm(one, BF), vm(one, BF), vm(half, BF), vm((64, D), BF),
        dma((POOL,)), dma((2, 16)), dma((16,)), dma((16,)), dma((2, 8, 2)), dma((2,)), dma((2, 18)), dma((2, 16)),
        dma((5,)), dma((2, 4)), dma((7,)),
    ]
    here = [pltpu.with_memory_space_constraint(v, pltpu.HBM) for v in (xin, *weights)]
    outs = pl.pallas_call(
        kernel,
        out_shape=tuple(pltpu.VMEM(o.shape, o.dtype) for o in out_shape),
        in_specs=[pl.BlockSpec(memory_space=pltpu.HBM)] * 9,
        out_specs=tuple(pl.BlockSpec(memory_space=pl.ANY) for _ in range(7)),
        scratch_shapes=scratch,
        compiler_params=pltpu.CompilerParams(
            collective_id=0, has_side_effects=True, vmem_limit_bytes=VMEM_MB * 1024 * 1024
        ),
    )(*here)
    return pl.pallas_call(
        copy_out,
        out_shape=out_shape,
        in_specs=[pl.BlockSpec(memory_space=pl.ANY)] * 7,
        out_specs=tuple(pl.BlockSpec(memory_space=pltpu.HBM) for _ in range(7)),
        scratch_shapes=[dma((7,))],
        compiler_params=pltpu.CompilerParams(vmem_limit_bytes=1024 * 1024),
    )(*outs)


def per_device(
    prompts, gain_first, gate_first, up_first, down_first, gain_second, gate_second, up_second, down_second
):
    xin = prompts.reshape(4, 4, 64, D)
    g1, u1, d1, g2, u2, d2, ps = run(
        xin,
        gain_first.reshape(1, 128), gate_first.T, up_first.T, down_first,
        gain_second.reshape(1, 128), gate_second.T, up_second.T, down_second,
    )
    return g1.T, u1.T, d1, g2.T, u2.T, d2, ps.reshape(1, 64, D)


def solution(mesh):
    w = P("fs", "tp")
    return jax.shard_map(
        per_device,
        mesh=mesh,
        in_specs=(P("tp", None, None), P("fs"), w, w, w, P("fs"), w, w, w),
        out_specs=(
            P(None, "fs"), P(None, "fs"), P("fs", None),
            P(None, "fs"), P(None, "fs"), P("fs", None),
            P("tp", "fs", None),
        ),
        check_vma=False,
    )
```

time: 125 us -> 120 us (0.960)
  Pallas kernels: 124 us -> 119 us
    pallas_call x1, Pallas kernels: 121 us -> 115 us  [run(): pl.pallas_call(kernel, out_shape=tuple((pltpu.VMEM(o.shape, o.dtype) for...]
where the time goes in v4:
time: 120 us; the launch traced here: 119 us
  Pallas kernels  119 us (99%)
    pallas_call x1, Pallas kernels, run(): pl.pallas_call(kernel, out_shape=tuple((pltpu.VMEM(o.shape, o.dtype) for...  115 us
    pallas_call x1, Pallas kernels, run(): pl.pallas_call(copy_out, out_shape=out_shape, in_specs=[pl.BlockSpec(memo...  3.49 us

profile of v4, /device:TPU:1, one launch (start us, length us, event | category | flops | bytes accessed | tf_op | source)
XLA Modules:
  0.0 119.3 jit_solution(16589689156926455179)
XLA Ops:
  0.6 115.0 %shard_map.144 = (bf16[352,2048]{1,0:T(8,128)(2,1)S(1)}, bf16[352,2048]{1,0:T(8,128)(2,1)S(1)}, bf16[352,2048]{1,0:T(8,128)(2,1)S(1)}, bf16[352,2048]{1,0:T(8,12...) custom-call(bf16[4,4,64,2048]{3,2,1,0:T(8,128)(2,1)} %bitcast.12, ...), custom_call_target="tpu_custom_call" | custom-call | tf_op jit(solution)/shard_map/pallas_call | solution.py:623
  115.7 3.5 %shard_map.145 = (bf16[352,2048]{1,0:T(8,128)(2,1)}, bf16[352,2048]{1,0:T(8,128)(2,1)}, bf16[352,2048]{1,0:T(8,128)(2,1)}, bf16[352,2048]{1,0:T(8,128)(2,1)}, bf...) custom-call(bf16[352,2048]{1,0:T(8,128)(2,1)S(1)} %get-tuple-element.21.refs_0_, ...), custom_call_target="tpu_custom_call" | custom-call | tf_op jit(solution)/shard_map/pallas_call | solution.py:633

commit v5 on v4

--- a/solution.py
+++ b/solution.py
@@ -16,7 +16,7 @@
 BF = jnp.bfloat16
 F32 = jnp.float32
 VMEM_MB = 53
-POOL = 64
+POOL = 56
 
 
 def rem4(v):
@@ -28,7 +28,7 @@
     g1_o, u1_o, d1_o, g2_o, u2_o, d2_o, ps_o,
     nx, ng, xown, mid, raw_w, raw_d, raw_g, wt, dn, gu, dd, act, part,
     gates, r2, ra, rb, tt, acc, sb, q2, qa, qb, qt, ost,
-    pool, w1_recv, w_recv, w_send, d_recv, d_loc, rs_recv, ag_recv, x_sem, i_sem, o_sem,
+    pool, w1_recv, w_recv, w_send, d_recv, d_loc, rs_recv, ag_recv, x_sem, i_sem,
 ):
     f = lax.axis_index("fs")
     t = lax.axis_index("tp")
@@ -447,11 +447,11 @@
 
     def ag_start():
         for ab in range(2):
-            own = gv(ab, 0, 0)
-            snd(ab, 0, own, False, 1)
-            snd(ab, 1, own, False, -1)
-            snd(ab, 4, own, True, 1)
-            snd(ab, 8, own, True, -1)
+            snd(ab, 0, gv(ab, 0, 0), False, 1)
+            snd(ab, 1, gv(ab, 0, 0), False, -1)
+        for ab in range(2):
+            snd(ab, 4, gv(ab, 0, 0), True, 1)
+            snd(ab, 8, gv(ab, 0, 0), True, -1)
 
     def ag_first():
         for ab in range(2):
@@ -459,6 +459,7 @@
             snd(ab, 2, gv(ab, 3, 0, lo_rows), False, 1)
             got(ab, 1)
             snd(ab, 3, gv(ab, 1, 0, hi_rows), False, -1)
+        for ab in range(2):
             snd(ab, 5, gv(ab, 1, 0), True, 1)
             snd(ab, 11, gv(ab, 3, 0), True, -1)
             snd(ab, 7, gv(ab, 3, 0), True, 1)
@@ -493,10 +494,10 @@
                 got(1, k)
 
     def put(src, dst, k):
-        pltpu.make_async_copy(src, dst, o_sem.at[k]).start()
+        pltpu.make_async_copy(src, dst, i_sem.at[k // 4, k % 4]).start()
 
     def put_wait(src, dst, k):
-        pltpu.make_async_copy(src, dst, o_sem.at[k]).wait()
+        pltpu.make_async_copy(src, dst, i_sem.at[k // 4, k % 4]).wait()
 
     def fold(h):
         for k in range(4):
@@ -547,8 +548,7 @@
         2: (lambda: act_row(0, z),),
         3: (lambda: hop(1, 0),),
         4: (lambda: hop(1, 1),),
-        5: (lambda: hop(2, 0),),
-        6: (lambda: d_own(1),),
+        5: (lambda: hop(2, 0), lambda: d_own(1)),
     })
     own_in.wait()
     m = (xown[...].astype(F32) + 0.5 * branch).astype(BF)
@@ -558,20 +558,21 @@
     hop(2, 1)
     ag_first()
     ag_second()
-    d_fwd(1)
     hop(3, 0)
     ag_third()
+    d_fwd(1)
+    ag_fourth()
     hop(3, 1)
     hop_end()
     ag_row(0)
     act_row(1, z)
-    ag_fourth()
     put(gu.at[1, 0, pl.ds(0, HB)], g2_o, 3)
     put(gu.at[1, 1, pl.ds(0, HB)], u2_o, 4)
     for oz in (1, 3):
         ag_row(oz)
         act_row(1, rem4(z + oz))
-    d_more(1)
+        if oz == 1:
+            d_more(1)
     ag_row(2)
     act_row(1, rem4(z + 2))
     d_end(1)
@@ -617,7 +618,7 @@
         vm(unit, BF), vm(unit, BF), vm(unit, BF), vm(unit, BF), vm((2, 4, 64, 1024), F32), vm(unit, BF),
         vm(half, BF), vm(one, BF), vm(one, BF), vm(half, BF), vm((64, D), BF),
         dma((POOL,)), dma((2, 16)), dma((16,)), dma((16,)), dma((2, 8, 2)), dma((2,)), dma((2, 18)), dma((2, 16)),
-        dma((5,)), dma((2, 4)), dma((7,)),
+        dma((5,)), dma((2, 4)),
     ]
     here = [pltpu.with_memory_space_constraint(v, pltpu.HBM) for v in (xin, *weights)]
     outs = pl.pallas_call(

time: 120 us -> 118 us (0.983)
  Pallas kernels: 119 us -> 116 us
    pallas_call x1, Pallas kernels: 115 us -> 113 us  [run(): pl.pallas_call(kernel, out_shape=tuple((pltpu.VMEM(o.shape, o.dtype) for...]
where the time goes in v5:
time: 118 us; the launch traced here: 117 us
  Pallas kernels  116 us (98%)
    pallas_call x1, Pallas kernels, run(): pl.pallas_call(kernel, out_shape=tuple((pltpu.VMEM(o.shape, o.dtype) for...  113 us
    pallas_call x1, Pallas kernels, run(): pl.pallas_call(copy_out, out_shape=out_shape, in_specs=[pl.BlockSpec(memo...  3.49 us

profile of v5, /device:TPU:1, one launch (start us, length us, event | category | flops | bytes accessed | tf_op | source)
XLA Modules:
  0.0 116.8 jit_solution(10388866587217128671)
XLA Ops:
  0.6 112.5 %shard_map.144 = (bf16[352,2048]{1,0:T(8,128)(2,1)S(1)}, bf16[352,2048]{1,0:T(8,128)(2,1)S(1)}, bf16[352,2048]{1,0:T(8,128)(2,1)S(1)}, bf16[352,2048]{1,0:T(8,12...) custom-call(bf16[4,4,64,2048]{3,2,1,0:T(8,128)(2,1)} %bitcast.12, ...), custom_call_target="tpu_custom_call" | custom-call | tf_op jit(solution)/shard_map/pallas_call | solution.py:624
  113.2 3.5 %shard_map.145 = (bf16[352,2048]{1,0:T(8,128)(2,1)}, bf16[352,2048]{1,0:T(8,128)(2,1)}, bf16[352,2048]{1,0:T(8,128)(2,1)}, bf16[352,2048]{1,0:T(8,128)(2,1)}, bf...) custom-call(bf16[352,2048]{1,0:T(8,128)(2,1)S(1)} %get-tuple-element.21.refs_0_, ...), custom_call_target="tpu_custom_call" | custom-call | tf_op jit(solution)/shard_map/pallas_call | solution.py:634

commit v6 on v5

--- a/solution.py
+++ b/solution.py
@@ -16,7 +16,7 @@
 BF = jnp.bfloat16
 F32 = jnp.float32
 VMEM_MB = 53
-POOL = 56
+POOL = 40
 
 
 def rem4(v):
@@ -28,7 +28,7 @@
     g1_o, u1_o, d1_o, g2_o, u2_o, d2_o, ps_o,
     nx, ng, xown, mid, raw_w, raw_d, raw_g, wt, dn, gu, dd, act, part,
     gates, r2, ra, rb, tt, acc, sb, q2, qa, qb, qt, ost,
-    pool, w1_recv, w_recv, w_send, d_recv, d_loc, rs_recv, ag_recv, x_sem, i_sem,
+    pool, w1_recv, w_recv, w_send, d_recv, d_loc, rs_recv, x_sem, i_sem,
 ):
     f = lax.axis_index("fs")
     t = lax.axis_index("tp")
@@ -397,7 +397,6 @@
             rs_turn(h, ab, 2)
             rs_direct(h, ab, 3)
             rs_turn(h, ab, 3)
-        point(3)
         for ab in (1, 0):
             rs_turn(h, ab, 1)
             rs_direct(h, ab, 1)
@@ -407,6 +406,7 @@
             rs_fin(h, ab, 2)
         for ab in (1, 0):
             rs_direct(h, ab, 0)
+        point(3)
         for ab in (1, 0):
             rs_fin(h, ab, 3)
             rs_turn(h, ab, 0)
@@ -440,10 +440,10 @@
         for k in slots:
             if (ab, k) not in waited:
                 waited.add((ab, k))
-                arrived(gv(ab, *LAND[k]), ag_recv.at[ab, k])
+                arrived(gv(ab, *LAND[k]), w1_recv.at[ab, k])
 
     def snd(ab, k, ref, second, step):
-        send(ref, ref, ag_recv.at[ab, k], dev1(ab if second else 1 - ab, step))
+        send(ref, ref, w1_recv.at[ab, k], dev1(ab if second else 1 - ab, step))
 
     def ag_start():
         for ab in range(2):
@@ -535,11 +535,11 @@
     gate_row(2)
     gate_row(3)
     w_end(1)
+    d_more(0)
     put(gu.at[0, 0, pl.ds(0, HB)], g1_o, 0)
     put(gu.at[0, 1, pl.ds(0, HB)], u1_o, 1)
     act_col(rem4(x + 2))
     act_row(0, rem4(z + 2))
-    d_more(0)
     d_end(0)
     put(dd.at[0, pl.ds(0, HB)], d1_o, 2)
     branch = rs_run(0, {
@@ -547,21 +547,21 @@
         1: (lambda: act_row(0, rem4(z + 1)),),
         2: (lambda: act_row(0, z),),
         3: (lambda: hop(1, 0),),
-        4: (lambda: hop(1, 1),),
-        5: (lambda: hop(2, 0), lambda: d_own(1)),
+        5: (lambda: hop(1, 1), lambda: d_own(1)),
     })
     own_in.wait()
     m = (xown[...].astype(F32) + 0.5 * branch).astype(BF)
     mid[...] = m
     ng[z, x] = norm_rows(m)
     ag_start()
+    hop(2, 0)
+    ag_first()
     hop(2, 1)
-    ag_first()
     ag_second()
-    hop(3, 0)
     ag_third()
     d_fwd(1)
     ag_fourth()
+    hop(3, 0)
     hop(3, 1)
     hop_end()
     ag_row(0)
@@ -617,7 +617,7 @@
         vm((4, 4, 64, HP), F32),
         vm(unit, BF), vm(unit, BF), vm(unit, BF), vm(unit, BF), vm((2, 4, 64, 1024), F32), vm(unit, BF),
         vm(half, BF), vm(one, BF), vm(one, BF), vm(half, BF), vm((64, D), BF),
-        dma((POOL,)), dma((2, 16)), dma((16,)), dma((16,)), dma((2, 8, 2)), dma((2,)), dma((2, 18)), dma((2, 16)),
+        dma((POOL,)), dma((2, 16)), dma((16,)), dma((16,)), dma((2, 8, 2)), dma((2,)), dma((2, 18)),
         dma((5,)), dma((2, 4)),
     ]
     here = [pltpu.with_memory_space_constraint(v, pltpu.HBM) for v in (xin, *weights)]

time: 118 us -> 117 us (level); the launches traced: 117 us -> 117 us
  no operation moved by 1% of the time
where the time goes in v6:
time: 117 us
  Pallas kernels  116 us (99%)
    pallas_call x1, Pallas kernels, run(): pl.pallas_call(kernel, out_shape=tuple((pltpu.VMEM(o.shape, o.dtype) for...  113 us
    pallas_call x1, Pallas kernels, run(): pl.pallas_call(copy_out, out_shape=out_shape, in_specs=[pl.BlockSpec(memo...  3.49 us

profile of v6, /device:TPU:1, one launch (start us, length us, event | category | flops | bytes accessed | tf_op | source)
XLA Modules:
  0.0 117.1 jit_solution(2334459283451218781)
XLA Ops:
  0.6 112.8 %shard_map.144 = (bf16[352,2048]{1,0:T(8,128)(2,1)S(1)}, bf16[352,2048]{1,0:T(8,128)(2,1)S(1)}, bf16[352,2048]{1,0:T(8,128)(2,1)S(1)}, bf16[352,2048]{1,0:T(8,12...) custom-call(bf16[4,4,64,2048]{3,2,1,0:T(8,128)(2,1)} %bitcast.12, ...), custom_call_target="tpu_custom_call" | custom-call | tf_op jit(solution)/shard_map/pallas_call | solution.py:624
  113.4 3.5 %shard_map.145 = (bf16[352,2048]{1,0:T(8,128)(2,1)}, bf16[352,2048]{1,0:T(8,128)(2,1)}, bf16[352,2048]{1,0:T(8,128)(2,1)}, bf16[352,2048]{1,0:T(8,128)(2,1)}, bf...) custom-call(bf16[352,2048]{1,0:T(8,128)(2,1)S(1)} %get-tuple-element.21.refs_0_, ...), custom_call_target="tpu_custom_call" | custom-call | tf_op jit(solution)/shard_map/pallas_call | solution.py:634

commit v7 on v6

--- a/solution.py
+++ b/solution.py
@@ -16,7 +16,7 @@
 BF = jnp.bfloat16
 F32 = jnp.float32
 VMEM_MB = 53
-POOL = 40
+POOL = 32
 
 
 def rem4(v):
@@ -571,8 +571,7 @@
     for oz in (1, 3):
         ag_row(oz)
         act_row(1, rem4(z + oz))
-        if oz == 1:
-            d_more(1)
+    d_more(1)
     ag_row(2)
     act_row(1, rem4(z + 2))
     d_end(1)

time: 117 us -> 117 us (level)
  no operation moved by 1% of the time
where the time goes in v7:
time: 117 us
  Pallas kernels  116 us (99%)
    pallas_call x1, Pallas kernels, run(): pl.pallas_call(kernel, out_shape=tuple((pltpu.VMEM(o.shape, o.dtype) for...  113 us
    pallas_call x1, Pallas kernels, run(): pl.pallas_call(copy_out, out_shape=out_shape, in_specs=[pl.BlockSpec(memo...  3.49 us

profile of v7, /device:TPU:1, one launch (start us, length us, event | category | flops | bytes accessed | tf_op | source)
XLA Modules:
  0.0 116.9 jit_solution(16267204355733925943)
XLA Ops:
  0.6 112.6 %shard_map.144 = (bf16[352,2048]{1,0:T(8,128)(2,1)S(1)}, bf16[352,2048]{1,0:T(8,128)(2,1)S(1)}, bf16[352,2048]{1,0:T(8,128)(2,1)S(1)}, bf16[352,2048]{1,0:T(8,12...) custom-call(bf16[4,4,64,2048]{3,2,1,0:T(8,128)(2,1)} %bitcast.12, ...), custom_call_target="tpu_custom_call" | custom-call | tf_op jit(solution)/shard_map/pallas_call | solution.py:623
  113.3 3.5 %shard_map.145 = (bf16[352,2048]{1,0:T(8,128)(2,1)}, bf16[352,2048]{1,0:T(8,128)(2,1)}, bf16[352,2048]{1,0:T(8,128)(2,1)}, bf16[352,2048]{1,0:T(8,128)(2,1)}, bf...) custom-call(bf16[352,2048]{1,0:T(8,128)(2,1)S(1)} %get-tuple-element.21.refs_0_, ...), custom_call_target="tpu_custom_call" | custom-call | tf_op jit(solution)/shard_map/pallas_call | solution.py:633
